TPU v7x, 512 devices: a whole 4x8x8 slice. The times are simulated.
512 devices in a mesh: rep: 2 (over z_hi), fs: 32 (over z_lo, y), tp: 8 (over x, core).
Axes of the slice: x: 4, y: 8, z: 8 (z_hi: 2, z_lo: 4; z = z_hi * 4 + z_lo), core: 2. Of those that a mesh axis runs over, the one named last changes fastest.
Arguments:
- residual: bfloat16 [2048, 16384], P('tp', ('rep', 'fs')), may hold values from -6 to 6
- mixer_gain: float32 [2048], replicated, may hold values from 0.1 to 1.9
- value_weight: float32 [2048, 512], P('fs', 'tp'), may hold values from -0.125 to 0.125
- value_scale: float32 [512], P('tp'), may hold values from 0.2 to 8, as said below
- input_gate_weight: float32 [2048, 512], P('fs', 'tp'), may hold values from -0.125 to 0.125
- input_gate_scale: float32 [512], P('tp'), may hold values from 0.5 to 2
- output_gate_weight: float32 [2048, 512], P('fs', 'tp'), may hold values from -0.125 to 0.125
- output_gate_scale: float32 [512], P('tp'), may hold values from 0.5 to 2
- conv_taps: float32 [3, 512], P(None, 'tp'), may hold values from -3 to 3
- conv_gain: float32 [512], P('tp'), may hold values from 0.1 to 1.9
- mixer_out_weight: float32 [512, 2048], P('tp', 'fs'), may hold values from -0.25 to 0.25
- mixer_out_scale: float32 [2048], P('fs'), may hold values from 0.5 to 2
- channel_gain: float32 [2048], replicated, may hold values from 0.1 to 1.9
- gate_weight: float32 [2048, 5632], P('fs', 'tp'), may hold values from -0.125 to 0.125
- gate_scale: float32 [5632], P('tp'), may hold values from 0.5 to 2
- up_weight: float32 [2048, 5632], P('fs', 'tp'), may hold values from -0.125 to 0.125
- up_scale: float32 [5632], P('tp'), may hold values from 0.5 to 2
- down_weight: float32 [5632, 2048], P('tp', 'fs'), may hold values from -0.078125 to 0.078125
- down_scale: float32 [2048], P('fs'), may hold values from 0.5 to 2
Outputs:
- layer_out: bfloat16 [2048, 16384], P('tp', ('rep', 'fs'))
Inputs may be any that keep to these rules, and one draw needn't show every extreme that they name: `value_scale`: positive column scales.
All inputs are finite; a program needn't handle non-finite values.
Results may differ from a plain program's by a relative error of at most 0.018.
Values may be sent and summed in bfloat16 or wider, within the bound.
A program may use at most 64 MiB of HBM per device.

v0:
```python
import jax
import jax.numpy as jnp
from jax import lax
from jax.sharding import Mesh
from jax.sharding import PartitionSpec as P

LEN = 128
FS = ("fs_0", "fs_1")
REP_FS = ("rep", "fs_0", "fs_1")


epsilon = 1e-06


def copy_for_each(value, axis):
    devices = lax.axis_size(axis)
    return lax.all_to_all(
        jnp.broadcast_to(value[None], (devices, *value.shape)), axis, 0, 0, tiled=True
    )


def in_order(tiles, dim):
    tiles = jnp.moveaxis(tiles, 0, dim)
    dims = tiles.shape
    return tiles.reshape(*dims[:dim], dims[dim] * dims[dim + 1], *dims[dim + 2 :])


def gathered_copies(value, axis, dim):
    tiles = copy_for_each(value, axis)
    return in_order(tiles, dim)


def sent_together(arrays, axis, dim, along):
    ends, at = ([], 0)
    for a in arrays[:-1]:
        at += a.shape[along]
        ends.append(at)
    both = jnp.concatenate(arrays, axis=along)
    return tuple(jnp.split(lax.all_gather(both, axis, axis=dim, tiled=True), ends, axis=along))


def of_everyone(value, axis):
    return copy_for_each(value, axis).sum(axis=0)


def gather_turned(arrays, axis, dims):
    turned = [jnp.moveaxis(a, dim, 0) for a, dim in zip(arrays, dims)]
    widths = [t[0].size for t in turned]
    both = jnp.concatenate([t.reshape(-1, w) for t, w in zip(turned, widths)], axis=1)
    result = lax.all_gather(both, axis, axis=0, tiled=True)
    tiles = jnp.split(result, [sum(widths[:k]) for k in range(1, len(widths))], axis=1)
    return tuple(
        (
            jnp.moveaxis(b.reshape(-1, *t.shape[1:]), 0, dim)
            for b, t, dim in zip(tiles, turned, dims)
        )
    )


def stacked_from(value, axes, order):
    tiles = value[None]
    for k in order:
        tiles = lax.all_gather(tiles, axes[k], axis=0, tiled=True)
    held = [lax.axis_size(axes[k]) for k in reversed(order)]
    tiles = tiles.reshape(*held, *value.shape)
    turned = sorted(range(len(order)), key=lambda place: order[len(order) - 1 - place])
    return tiles.transpose(*turned, *range(len(order), tiles.ndim)).reshape(-1, *value.shape)


def whole_of(value, axes, order, dim):
    return in_order(stacked_from(value, axes, order), dim)


def split_up(value, dim, devices):
    dims = value.shape
    tiles = value.reshape(*dims[:dim], devices, dims[dim] // devices, *dims[dim + 1 :])
    return jnp.moveaxis(tiles, dim, 0)


def sum_at_owner(value, axis, dim):
    tiles = split_up(value, dim, lax.axis_size(axis))
    arrived = lax.all_to_all(tiles, axis, split_axis=0, concat_axis=0, tiled=True)
    return arrived.astype(jnp.float32).sum(axis=0)


def normalize(values, gain):
    floats = values.astype(jnp.float32)
    mean = jnp.mean(floats * floats, axis=0, keepdims=True)
    return (floats * lax.rsqrt(mean + epsilon) * gain[:, None]).astype(jnp.bfloat16)


def contract(weight, rows):
    return lax.dot_general(
        weight, rows, (((0,), (0,)), ((), ())), preferred_element_type=jnp.float32
    )


def causal_conv(values, taps, length):
    total = values.shape[1]
    position = jnp.arange(total, dtype=jnp.int32) % length
    shifted_one = jnp.pad(values, ((0, 0), (1, 0)))[:, :total]
    shifted_two = jnp.pad(values, ((0, 0), (2, 0)))[:, :total]
    shifted_one = jnp.where(position[None, :] >= 1, shifted_one, 0.0)
    shifted_two = jnp.where(position[None, :] >= 2, shifted_two, 0.0)
    return (
        taps[2][:, None] * values + taps[1][:, None] * shifted_one + taps[0][:, None] * shifted_two
    )


def local(
    residual,
    mixer_gain,
    value_weight,
    value_scale,
    input_gate_weight,
    input_gate_scale,
    output_gate_weight,
    output_gate_scale,
    conv_taps,
    conv_gain,
    mixer_out_weight,
    mixer_out_scale,
    channel_gain,
    gate_weight,
    gate_scale,
    up_weight,
    up_scale,
    down_weight,
    down_scale,
):
    own_rows = residual.shape[0]
    tokens = residual.shape[1]
    groups = lax.axis_size("tp")
    channels = value_weight.shape[1] * groups
    whole = gathered_copies(residual, "tp", 0)
    normed = normalize(whole, mixer_gain)
    pieces = sent_together(
        (
            value_weight.astype(jnp.bfloat16),
            input_gate_weight.astype(jnp.bfloat16),
            output_gate_weight.astype(jnp.bfloat16),
        ),
        FS,
        0,
        1,
    )
    value = contract(pieces[0], normed)
    in_gate = contract(pieces[1], normed)
    out_gate = contract(pieces[2], normed)
    value = value * value_scale[:, None]
    in_gate = in_gate * input_gate_scale[:, None]
    out_gate = out_gate * output_gate_scale[:, None]
    mixed = out_gate * causal_conv(in_gate * value, conv_taps, LEN)
    squares = of_everyone(jnp.sum(mixed * mixed, axis=0), "tp")
    conv_normed = (
        mixed * lax.rsqrt(squares / channels + epsilon)[None, :] * conv_gain[:, None]
    ).astype(jnp.bfloat16)
    out_full = gathered_copies(mixer_out_weight.astype(jnp.bfloat16), FS, 1)
    out_scale, down_scale_full = gather_turned((mixer_out_scale, down_scale), FS, (0, 0))
    conv_all = gathered_copies(conv_normed, "tp", 0)
    out_own = lax.all_to_all(out_full, "tp", split_axis=1, concat_axis=0, tiled=True)
    block_width = conv_normed.shape[0]
    weight_blocks = out_own.reshape(groups, block_width, own_rows)
    row_blocks = conv_all.reshape(groups, block_width, tokens)
    parts = lax.dot_general(
        weight_blocks, row_blocks, (((1,), (1,)), ((0,), (0,))), preferred_element_type=jnp.float32
    )
    own_scale = lax.dynamic_slice_in_dim(out_scale, lax.axis_index("tp") * own_rows, own_rows, 0)
    rounded = (parts * own_scale[None, :, None]).astype(jnp.bfloat16)
    total = jnp.sum(rounded.astype(jnp.float32), axis=0)
    after_own = (residual.astype(jnp.float32) + total).astype(jnp.bfloat16)
    after_whole = gathered_copies(after_own, "tp", 0)
    normed_two = normalize(after_whole, channel_gain)
    gate_full, up_full = sent_together(
        (gate_weight.astype(jnp.bfloat16), up_weight.astype(jnp.bfloat16)), FS, 0, 1
    )
    gate = contract(gate_full, normed_two)
    upper = contract(up_full, normed_two)
    hidden = (jax.nn.silu(gate * gate_scale[:, None]) * (upper * up_scale[:, None])).astype(
        jnp.bfloat16
    )
    down_full = whole_of(down_weight.astype(jnp.bfloat16), FS, (0, 1), 1)
    total_two = sum_at_owner(
        (contract(down_full, hidden) * down_scale_full[:, None]).astype(jnp.bfloat16), "tp", 0
    )
    return (after_own.astype(jnp.float32) + total_two).astype(jnp.bfloat16)


def solution(mesh):
    torus = Mesh(
        mesh.devices.reshape(mesh.shape["rep"], 4, 8, mesh.shape["tp"]),
        ("rep", "fs_0", "fs_1", "tp"),
    )
    in_specs = (
        P("tp", REP_FS),
        P(),
        P(FS, "tp"),
        P("tp"),
        P(FS, "tp"),
        P("tp"),
        P(FS, "tp"),
        P("tp"),
        P(None, "tp"),
        P("tp"),
        P("tp", FS),
        P(FS),
        P(),
        P(FS, "tp"),
        P("tp"),
        P(FS, "tp"),
        P("tp"),
        P("tp", FS),
        P(FS),
    )
    out_specs = P("tp", REP_FS)
    return jax.shard_map(local, mesh=torus, in_specs=in_specs, out_specs=out_specs, check_vma=False)
```

profile of v0, /device:TPU:1, one launch (start us, length us, event | category | flops | bytes accessed | tf_op | source)
XLA Modules:
  0.0 313.9 jit_solution(3296129900674847055)
XLA Ops:
  6.5 1.0 convert_bitcast_fusion
  7.5 17.1 %all-gather.2 = bf16[4,704,64]{1,2,0:T(8,128)(2,1)} all-gather(bf16[1,704,64]{1,2,0:T(8,128)(2,1)S(1)} %convert_bitcast_fusion), channel_id=2, replica_groups=mesh['rep'=2,'fs_0'=4,'fs_1'=8,'tp'=8] {'fs_0'}, dimensions={0}, use_global_device_ids=true | all-gather | bytes 450560 | tf_op jit(solution)/shard_map/all_gather | solution.py:63
  24.6 0.9 convert_element_type.99
  25.6 1.0 convert_element_type.98
  26.6 0.8 pad_maximum_fusion
  27.4 1.0 broadcast_in_dim.30
  28.4 9.1 %all-to-all-start = ((bf16[8,256,256]{2,1,0:T(8,128)(2,1)}), bf16[8,256,256]{2,1,0:T(8,128)(2,1)S(1)}, u32[]{:S(2)}, u32[]{:S(2)}) async-start(bf16[8,256,256]{2,1,0:T(8,128)(2,1)} %broadcast_in_dim.30), calls=%async_computation | async-start | bytes 2097152 | tf_op jit(solution)/shard_map/all_to_all | solution.py:17
  37.7 1.1 reshape.106
  39.0 77.3 %all_gather.15 = bf16[2048,192]{1,0:T(8,128)(2,1)S(1)} all-gather(bf16[64,192]{1,0:T(8,128)(2,1)S(1)} %pad_maximum_fusion.1), channel_id=1, replica_groups=mesh['rep'=2,'fs_0'=4,'fs_1'=8,'tp'=8] {'fs_0','fs_1'}, dimensions={0}, use_global_device_ids=true | all-gather | bytes 811008 | tf_op jit(solution)/shard_map/all_gather | solution.py:39
  116.3 4.0 %all-to-all-start.3 = ((bf16[32,2,2048]{2,1,0:T(2,128)(2,1)}), bf16[32,2,2048]{2,1,0:T(2,128)(2,1)S(1)}, u32[]{:S(2)}, u32[]{:S(2)}) async-start(bf16[32,2,2048]{2,1,0:T(2,128)(2,1)} %reshape.106), calls=%async_computation.3 | async-start | bytes 524288 | tf_op jit(solution)/shard_map/all_to_all | solution.py:17
  121.0 0.5 convolution_multiply_fusion.2
  122.2 9.0 %all-to-all-done.3 = bf16[32,2,2048]{2,1,0:T(2,128)(2,1)S(1)} async-done(((bf16[32,2,2048]{2,1,0:T(2,128)(2,1)}), bf16[32,2,2048]{2,1,0:T(2,128)(2,1)S(1)}, u32[]{:S(2)}, u32[]{:S(2)}) %all-to-all-start.3) | async-done | bytes 262176 | tf_op jit(solution)/shard_map/all_to_all | solution.py:17
  131.2 0.6 broadcast_in_dim.34
  131.8 19.3 %all-to-all-start.1 = ((f32[8,1,256]{2,1,0:T(1,128)}), f32[8,1,256]{2,1,0:T(1,128)S(1)}, u32[]{:S(2)}, u32[]{:S(2)}) async-start(f32[8,1,256]{2,1,0:T(1,128)} %broadcast_in_dim.34), calls=%async_computation.1 | async-start | bytes 16384 | tf_op jit(solution)/shard_map/all_to_all | solution.py:17
  151.2 64.4 %all-gather.1 = f32[32,64,2]{1,2,0:T(2,128)S(1)} all-gather(f32[1,64,2]{1,2,0:T(2,128)S(1)} %maximum_bitcast_fusion), channel_id=1, replica_groups=mesh['rep'=2,'fs_0'=4,'fs_1'=8,'tp'=8] {'fs_0','fs_1'}, dimensions={0}, use_global_device_ids=true | all-gather | bytes 16896 | tf_op jit(solution)/shard_map/all_gather | solution.py:50
  215.7 0.4 reshape.107
  216.1 0.3 copy.45
  216.8 0.8 copy.46
  217.5 15.9 %all-to-all-start.4 = ((bf16[64,8,256]{2,0,1:T(8,128)(2,1)}), bf16[64,8,256]{2,0,1:T(8,128)(2,1)S(1)}, u32[]{:S(2)}, u32[]{:S(2)}) async-start(bf16[64,8,256]{2,0,1:T(8,128)(2,1)} %copy.46), calls=%async_computation.4 | async-start | bytes 524288 | tf_op jit(solution)/shard_map/all_to_all | solution.py:161
  233.6 6.6 %all-to-all-done.4 = bf16[64,8,256]{2,0,1:T(8,128)(2,1)S(1)} async-done(((bf16[64,8,256]{2,0,1:T(8,128)(2,1)}), bf16[64,8,256]{2,0,1:T(8,128)(2,1)S(1)}, u32[]{:S(2)}, u32[]{:S(2)}) %all-to-all-start.4) | async-done | bytes 262176 | tf_op jit(solution)/shard_map/all_to_all | solution.py:161
  240.2 0.7 broadcast_in_dim.35
  240.9 4.1 %all-to-all-start.2 = ((bf16[8,64,256]{2,1,0:T(8,128)(2,1)}), bf16[8,64,256]{2,1,0:T(8,128)(2,1)S(1)}, u32[]{:S(2)}, u32[]{:S(2)}) async-start(bf16[8,64,256]{2,1,0:T(8,128)(2,1)} %broadcast_in_dim.35), calls=%async_computation.2 | async-start | bytes 524288 | tf_op jit(solution)/shard_map/all_to_all | solution.py:17
  245.2 6.3 %all-to-all-done.2 = bf16[8,64,256]{2,1,0:T(8,128)(2,1)S(1)} async-done(((bf16[8,64,256]{2,1,0:T(8,128)(2,1)}), bf16[8,64,256]{2,1,0:T(8,128)(2,1)S(1)}, u32[]{:S(2)}, u32[]{:S(2)}) %all-to-all-start.2) | async-done | bytes 262176 | tf_op jit(solution)/shard_map/all_to_all | solution.py:17
  251.5 0.5 convert_reduce_fusion.1
  252.3 18.4 %all_to_all.47 = bf16[8,256,256]{2,1,0:T(8,128)(2,1)S(1)} all-to-all(bf16[8,256,256]{2,1,0:T(8,128)(2,1)S(1)} %broadcast_in_dim.37), channel_id=1, replica_groups=mesh['rep'=2,'fs_0'=4,'fs_1'=8,'tp'=8] {'tp'}, dimensions={0} | all-to-all | bytes 2097152 | tf_op jit(solution)/shard_map/all_to_all | solution.py:17
  271.0 1.3 fusion.6
  272.3 2.1 copy.49
  274.5 4.0 %fusion.9 = f32[704,256]{1,0:T(8,128)} fusion(bf16[2048,256]{1,0:T(8,128)(2,1)} %fusion.6, bf16[2048,1408]{1,0:T(8,128)(2,1)} %all-gather.6.cloned.1.call-done, f32[704]{0:T(1024)S(1)} %copy-done.14), kind=kOutput, calls=%fused_computation.17 | convolution fusion | flops 738377728 | bytes 4918016 | tf_op jit(solution)/shard_map/dot_general | solution.py:93
  278.5 7.9 %fusion.4 = bf16[256,2048]{1,0:T(8,128)(2,1)} fusion(bf16[704,2048]{0,1:T(8,128)(2,1)S(1)} %bitcast.58, f32[2048]{0:T(1024)S(1)} %bitcast.61, bf16[2048,256]{1,0:T(8,128)(2,1)} %fusion.6, bf16[2048,1408]{1,0:T(8,128)(2,1)} %all-gather.6.cloned.1.call-done, f32[704,256]{1,0:T(8,128)} %fusion.9, f32[704]{0:T(1024)S(1)} %copy-done.15), kind=kOutput, calls=%fused_computation.5 | convolution fusion | flops 1478705152 | bytes 8858368 | tf_op jit(solution)/shard_map/dot_general | solution.py:93
  286.4 1.3 copy.57
  287.7 18.4 %all_to_all.48 = bf16[8,256,256]{1,2,0:T(8,128)(2,1)S(1)} all-to-all(bf16[8,256,256]{1,2,0:T(8,128)(2,1)S(1)} %bitcast.56), channel_id=1, replica_groups=mesh['rep'=2,'fs_0'=4,'fs_1'=8,'tp'=8] {'tp'}, dimensions={0} | all-to-all | bytes 2097152 | tf_op jit(solution)/shard_map/all_to_all | solution.py:82
  306.3 0.8 copy.52
  (70 shorter events, 3.1 us)
Async XLA Ops:
  6.5 20.8 %copy-start = (bf16[256,256]{1,0:T(8,128)(2,1)S(1)}, bf16[256,256]{1,0:T(8,128)(2,1)}, u32[]{:S(2)}) copy-start(bf16[256,256]{1,0:T(8,128)(2,1)} %param.19) | copy-start | bytes 393220
  6.5 265.8 %all-gather.8.cloned.1.call-start = ((), (), s32[]{:S(2)}) async-start(), calls=%async_computation.8 | async-start | bytes 3538944 | tf_op jit(solution)/shard_map/all_gather | solution.py:63
  24.6 249.9 %all-gather.6.cloned.1.call-start = ((), (), s32[]{:S(2)}) async-start(), calls=%async_computation.7 | async-start | bytes 5947392 | tf_op jit(solution)/shard_map/all_gather | solution.py:39
  25.6 11.9 %copy-start.1 = (f32[64,64]{1,0:T(8,128)S(1)}, f32[64,64]{1,0:T(8,128)}, u32[]{:S(2)}) copy-start(f32[64,64]{1,0:T(8,128)} %param.25) | copy-start | bytes 49156
  25.6 11.9 %copy-start.2 = (f32[64,64]{1,0:T(8,128)S(1)}, f32[64,64]{1,0:T(8,128)}, u32[]{:S(2)}) copy-start(f32[64,64]{1,0:T(8,128)} %param.23) | copy-start | bytes 49156
  25.6 11.9 %copy-start.3 = (f32[64,64]{1,0:T(8,128)S(1)}, f32[64,64]{1,0:T(8,128)}, u32[]{:S(2)}) copy-start(f32[64,64]{1,0:T(8,128)} %param.21) | copy-start | bytes 49156
  25.6 12.0 %copy-start.4 = (f32[64,64]{1,0:T(8,128)S(1)}, f32[64,64]{1,0:T(8,128)}, u32[]{:S(2)}) copy-start(f32[64,64]{1,0:T(8,128)} %param.29) | copy-start | bytes 49156
  28.4 10.4 %copy-start.12 = (f32[64]{0:T(128)S(1)}, f32[64]{0:T(128)}, u32[]{:S(2)}) copy-start(f32[64]{0:T(128)} %param.37) | copy-start | bytes 772
  28.4 10.4 %copy-start.13 = (f32[64]{0:T(128)S(1)}, f32[64]{0:T(128)}, u32[]{:S(2)}) copy-start(f32[64]{0:T(128)} %param.30) | copy-start | bytes 772
  28.4 10.5 %copy-start.7 = (f32[3,64]{1,0:T(4,128)S(1)}, f32[3,64]{1,0:T(4,128)}, u32[]{:S(2)}) copy-start(f32[3,64]{1,0:T(4,128)} %param.27) | copy-start | bytes 2308
  28.4 87.8 %all-to-all-start = ((bf16[8,256,256]{2,1,0:T(8,128)(2,1)}), bf16[8,256,256]{2,1,0:T(8,128)(2,1)S(1)}, u32[]{:S(2)}, u32[]{:S(2)}) async-start(bf16[8,256,256]{2,1,0:T(8,128)(2,1)} %broadcast_in_dim.30), calls=%async_computation | async-start | bytes 2097152 | tf_op jit(solution)/shard_map/all_to_all | solution.py:17
  37.6 83.0 %copy-start.5 = (f32[2048]{0:T(1024)S(1)}, f32[2048]{0:T(1024)}, u32[]{:S(2)}) copy-start(f32[2048]{0:T(1024)} %param.20) | copy-start | bytes 24580
  116.3 4.7 %copy-start.9 = (f32[64]{0:T(128)S(1)}, f32[64]{0:T(128)}, u32[]{:S(2)}) copy-start(f32[64]{0:T(128)} %param.24) | copy-start | bytes 772
  116.3 15.0 %all-to-all-start.3 = ((bf16[32,2,2048]{2,1,0:T(2,128)(2,1)}), bf16[32,2,2048]{2,1,0:T(2,128)(2,1)S(1)}, u32[]{:S(2)}, u32[]{:S(2)}) async-start(bf16[32,2,2048]{2,1,0:T(2,128)(2,1)} %reshape.106), calls=%async_computation.3 | async-start | bytes 524288 | tf_op jit(solution)/shard_map/all_to_all | solution.py:17
  120.6 0.9 copy-start.8
  121.0 0.9 copy-start.10
  122.2 111.3 %copy-start.11 = (f32[64]{0:T(128)S(1)}, f32[64]{0:T(128)}, u32[]{:S(2)}) copy-start(f32[64]{0:T(128)} %param.28) | copy-start | bytes 772
  131.8 85.7 %all-to-all-start.1 = ((f32[8,1,256]{2,1,0:T(1,128)}), f32[8,1,256]{2,1,0:T(1,128)S(1)}, u32[]{:S(2)}, u32[]{:S(2)}) async-start(f32[8,1,256]{2,1,0:T(1,128)} %broadcast_in_dim.34), calls=%async_computation.1 | async-start | bytes 16384 | tf_op jit(solution)/shard_map/all_to_all | solution.py:17
  217.5 22.6 %all-to-all-start.4 = ((bf16[64,8,256]{2,0,1:T(8,128)(2,1)}), bf16[64,8,256]{2,0,1:T(8,128)(2,1)S(1)}, u32[]{:S(2)}, u32[]{:S(2)}) async-start(bf16[64,8,256]{2,0,1:T(8,128)(2,1)} %copy.46), calls=%async_computation.4 | async-start | bytes 524288 | tf_op jit(solution)/shard_map/all_to_all | solution.py:161
  240.9 10.6 %all-to-all-start.2 = ((bf16[8,64,256]{2,1,0:T(8,128)(2,1)}), bf16[8,64,256]{2,1,0:T(8,128)(2,1)S(1)}, u32[]{:S(2)}, u32[]{:S(2)}) async-start(bf16[8,64,256]{2,1,0:T(8,128)(2,1)} %broadcast_in_dim.35), calls=%async_computation.2 | async-start | bytes 524288 | tf_op jit(solution)/shard_map/all_to_all | solution.py:17
  252.2 18.8 %copy-start.6 = (f32[2048]{0:T(1024)S(1)}, f32[2048]{0:T(1024)}, u32[]{:S(2)}) copy-start(f32[2048]{0:T(1024)} %param.31) | copy-start | bytes 24580
  272.3 2.2 copy-start.14
  274.4 4.1 %copy-start.15 = (f32[704]{0:T(1024)S(1)}, f32[704]{0:T(1024)}, u32[]{:S(2)}) copy-start(f32[704]{0:T(1024)} %param.35) | copy-start | bytes 8452
Sparse Core Ops, SparseCore 0:
  24.7 57.6 all-gather.7
  84.5 143.2 all-gather.5
where the time goes:
time: 315 us; the launch traced here: 314 us
  blocking collectives  196 us (62%)
  starting transfers between devices  52.5 us (17%)
  waiting for transfers between devices  22 us (7%)
  between operations  13.8 us (4%)
  matrix products  13.6 us (4%)
  local copies, waits for them, and re-layouts  10 us (3%)
  other arithmetic  6.34 us (2%)
    all_gather x1, blocking collectives, sent_together(): lax.all_gather(both, axis, axis=dim, tiled=True)  77.3 us
    all_gather x1, blocking collectives, gather_turned(): result = lax.all_gather(both, axis, axis=0, tiled=True)  64.4 us
    all_to_all x4, starting transfers between devices, copy_for_each(): lax.all_to_all(jnp.broadcast_to(value[None], (devices, *value.shape)), ax...  36.6 us
    all_to_all x1, blocking collectives, copy_for_each(): lax.all_to_all(jnp.broadcast_to(value[None], (devices, *value.shape)), ax...  18.4 us
    all_to_all x1, blocking collectives, sum_at_owner(): lax.all_to_all(tiles, axis, split_axis=0, concat_axis=0, tiled=True)  18.4 us
    all_gather x1, blocking collectives, stacked_from(): tiles = lax.all_gather(tiles, axes[k], axis=0, tiled=True)  17.1 us
    all_to_all x1, starting transfers between devices, local(): lax.all_to_all(out_full, 'tp', split_axis=1, concat_axis=0, tiled=True)  15.9 us
    all_to_all x4, waiting for transfers between devices, copy_for_each(): lax.all_to_all(jnp.broadcast_to(value[None], (devices, *value.shape)), ax...  15.4 us
  transfers between devices with their start and end apart: 7, of which 3 were waited for; matrix products, arithmetic and copies ran while one was open for 5% of the time, Pallas kernels for 0%

commit v1 on v0

v1 whole, which is shorter than its diff:
```python
import functools

import jax
import jax.numpy as jnp
from jax import lax
from jax.experimental import pallas as pl
from jax.experimental.pallas import tpu as pltpu
from jax.sharding import PartitionSpec as P

MESH = pl.DeviceIdType.MESH
F32 = jnp.float32
BF = jnp.bfloat16
EPS = 1e-06
LEN = 128
T = 256
NM, NG, ND = 256, 1408, 768
FFL = 704
ST = 272


class Event:
    def __init__(self, name, link, size, deps, put, got):
        self.name, self.link, self.size, self.deps = name, link, size, deps
        self.put, self.got = put, got


RATE = {"p": 300.0, "xx": 23.0}
LAT = {"p": 1.0, "xx": 2.6}


def plan(events, tasks):
    done, order, sent, flights = set(), [], set(), []
    free = {}
    now = 0.0

    def launch():
        for e in events:
            if e.name not in sent and all(d in done for d in e.deps):
                sent.add(e.name)
                start = max(now, free.get(e.link, 0.0))
                end = start + e.size / (RATE.get(e.link, 46.0) * 1e3)
                free[e.link] = end
                flights.append((end + LAT.get(e.link, 1.8), e))
                order.append(("send", e))

    launch()
    left = list(tasks)
    while flights or left:
        ready = [t for t in left if all(d in done for d in t[1])]
        landed = [f for f in flights if f[0] <= now]
        if landed:
            f = min(landed, key=lambda v: v[0])
        elif ready:
            t = ready[0]
            left.remove(t)
            order.append(("run", t))
            now += t[2]
            done.add(t[0])
            launch()
            continue
        else:
            f = min(flights, key=lambda v: v[0])
            now = f[0]
        flights.remove(f)
        order.append(("wait", f[1]))
        done.add(f[1].name)
        launch()
    return order


def weight_events(M, D, G, W):
    ev = []

    def add(name, link, size, deps, ref):
        ev.append(Event(name, link, size, deps, lambda: ref(*W.shift[link]), lambda: ref(0, 0)))

    def along_z(tag, buf, width, b, have, first):
        size = 64 * width * 2
        for sign, link in ((-1, "z+"), (1, "z-")):
            add(f"{tag}{link}1", link, size, have, lambda dz, dy, s=sign: buf.at[W.zl(s + dz), W.yy(b + dy)])
        for sign, link, lo in ((-1, "z+", 0), (1, "z-", 32)):
            add(f"{tag}{link}2", link, size // 2, [f"{tag}{link}1"],
                lambda dz, dy, s=sign, lo=lo: buf.at[W.zl(2 * s + dz), W.yy(b + dy), pl.ds(lo, 32)])
        return [f"{tag}z+1", f"{tag}z-1", f"{tag}z+2", f"{tag}z-2"]

    mz = along_z("M", M, NM, 0, ["initM"], True)
    all_m = list(mz)
    for s in (1, 2, 3, 4):
        for sign, link, lo in ((-1, "y+", 0), (1, "y-", 2)):
            deps = mz + ["initM"] if s == 1 else [f"My{link}{s - 1}"]
            n = 4 if s < 4 else 2
            at = 0 if s < 4 else lo
            add(f"My{link}{s}", link, n * 64 * NM * 2, deps,
                lambda dz, dy, s=s, sign=sign, at=at, n=n: M.at[pl.ds(at, n), W.yy(sign * s + dy)])
            all_m.append(f"My{link}{s}")
    all_g = []
    for s in (1, 2, 3, 4):
        for sign, link, lo in ((-1, "y+", 0), (1, "y-", 32)):
            deps = ["initG"] if s == 1 else [f"Gy{link}{s - 1}"]
            n = 64 if s < 4 else 32
            at = 0 if s < 4 else lo
            add(f"Gy{link}{s}", link, n * NG * 2, deps,
                lambda dz, dy, s=s, sign=sign, at=at, n=n: G.at[W.zl(dz), W.yy(sign * s + dy), pl.ds(at, n)])
            all_g.append(f"Gy{link}{s}")
    for b in (0, -1, 1, -2, 2, -3, 3, 4):
        if b == 0:
            have = ["initG"]
        elif b == 4:
            have = ["Gyy+4", "Gyy-4"]
        else:
            have = [f"Gyy+{-b}"] if b < 0 else [f"Gyy-{b}"]
        all_g += along_z(f"G{b}", G, NG, b, have, False)
    all_d = along_z("D", D, ND, 0, ["initD"], True)
    dz_names = list(all_d)
    for s in (1, 2, 3, 4):
        for g in (0, 1):
            for sign, link in ((-1, "y+"), (1, "y-")):
                if s == 4 and (g == 0) != (link == "y+"):
                    continue
                deps = dz_names + ["initD"] if s == 1 else [f"Dy{link}{s - 1}g{g}"]
                add(f"Dy{link}{s}g{g}", link, 2 * 64 * ND * 2, deps,
                    lambda dz, dy, s=s, sign=sign, g=g: D.at[pl.ds(2 * g, 2), W.yy(sign * s + dy)])
                all_d.append(f"Dy{link}{s}g{g}")
    return ev, all_m, all_g, all_d


class Where:
    pass


def kernel(m_in, g_in, d_in, xt_in, res, small, gus, gains, out,
           M, G, D, X1, X2, XN, acc, hid, keep, own32, preo, prei, rxo, rxi, qo, qi, ro, ri,
           send_sem, recv_sem, loc_sem, n_events):
    rep, fs, tp = lax.axis_index("rep"), lax.axis_index("fs"), lax.axis_index("tp")
    y, zl = lax.rem(fs, 8), lax.div(fs, 8)
    x, c = lax.div(tp, 2), lax.rem(tp, 2)
    z = rep * 4 + zl

    def y_at(d):
        return {"fs": zl * 8 + lax.rem(y + d + 8, 8)}

    def z_at(d):
        zz = lax.rem(z + d + 8, 8)
        return {"rep": lax.div(zz, 4), "fs": lax.rem(zz, 4) * 8 + y}

    def x_at(d):
        return {"tp": lax.rem(x + d + 4, 4) * 2 + c}

    partner = {"tp": x * 2 + 1 - c}
    target = {"y+": y_at(1), "y-": y_at(-1), "z+": z_at(1), "z-": z_at(-1),
              "x+": x_at(1), "x-": x_at(-1), "xx": x_at(2), "p": partner}

    W = Where()
    W.shift = {"y+": (0, 1), "y-": (0, -1), "z+": (1, 0), "z-": (-1, 0)}
    W.shift = {"y+": (0, 1), "y-": (0, -1), "z+": (1, 0), "z-": (-1, 0)}
    W.zl = lambda d: lax.rem(zl + d + 8, 4)
    W.yy = lambda d: lax.rem(y + d + 16, 8)

    ev, all_m, all_g, all_d = weight_events(M, D, G, W)
    pos = {"x+": -1, "x-": 1, "xx": 2}

    def slot(d, core):
        return lax.rem(x + d + 4, 4) * 2 + core

    def spread(tag, buf, first):
        names = []
        for link in ("x+", "x-", "xx"):
            ev.append(Event(f"{tag}{link}", link, T * 256 * 2, [first],
                            lambda: buf.at[slot(0, c)], lambda link=link: buf.at[slot(pos[link], c)]))
            names.append(f"{tag}{link}")
        ev.append(Event(f"{tag}p", "p", T * 256 * 2, [first],
                        lambda: buf.at[slot(0, c)], lambda: buf.at[slot(0, 1 - c)]))
        names.append(f"{tag}p")
        for link in ("x+", "x-", "xx"):
            ev.append(Event(f"{tag}p{link}", "p", T * 256 * 2, [f"{tag}{link}"],
                            lambda link=link: buf.at[slot(pos[link], c)],
                            lambda link=link: buf.at[slot(pos[link], 1 - c)]))
            names.append(f"{tag}p{link}")
        return names

    all_x1 = spread("X1", X1, "initX")
    hop = {"x+": 1, "x-": 3, "xx": 2}
    ev.append(Event("Q", "p", 4 * ST * T * 2, ["mix"], lambda: preo, lambda: prei))
    for link, j in hop.items():
        ev.append(Event(f"R{link}", link, ST * T * 2, ["mixsum"],
                        lambda j=j: rxo.at[j - 1], lambda j=j: rxi.at[j - 1]))
    all_x2 = spread("X2", X2, "after")
    for j in range(4):
        ev.append(Event(f"S{j}", "p", 256 * T * 2, [f"down{j}"], lambda j=j: qo.at[j], lambda j=j: qi.at[j]))
    for link, j in hop.items():
        ev.append(Event(f"U{link}", link, 256 * T * 2, [f"sum{j}"],
                        lambda j=j: ro.at[j - 1], lambda j=j: ri.at[j - 1]))
    assert len(ev) == n_events, len(ev)
    index = {e.name: i for i, e in enumerate(ev)}

    barrier = pltpu.get_barrier_semaphore()
    for dev in target.values():
        pl.semaphore_signal(barrier, inc=1, device_id=dev, device_id_type=MESH)

    def local_copy(i, src, dst):
        return pltpu.make_async_copy(src, dst, loc_sem.at[i])

    inits = [local_copy(0, m_in, M.at[zl, y]), local_copy(1, g_in, G.at[zl, y]),
             local_copy(2, d_in, D.at[zl, y]), local_copy(3, xt_in, X1.at[slot(0, c)])]
    for i in inits:
        i.start()
    for i in inits:
        i.wait()
    pl.semaphore_wait(barrier, 8)

    def start(e):
        i = index[e.name]
        ref = e.put()
        pltpu.make_async_remote_copy(src_ref=ref, dst_ref=ref if e.link[0] in "yz" or e.name[:1] == "X" else e.got(),
                                     send_sem=send_sem.at[i], recv_sem=recv_sem.at[i],
                                     device_id=target[e.link], device_id_type=MESH).start()

    def arrive(e):
        i = index[e.name]
        ref = e.got()
        pltpu.make_async_remote_copy(src_ref=ref, dst_ref=ref, send_sem=send_sem.at[i], recv_sem=recv_sem.at[i],
                                     device_id=target[e.link], device_id_type=MESH).wait_recv()

    def left(e):
        i = index[e.name]
        ref = e.put()
        pltpu.make_async_remote_copy(src_ref=ref, dst_ref=ref, send_sem=send_sem.at[i], recv_sem=recv_sem.at[i],
                                     device_id=target[e.link], device_id_type=MESH).wait_send()

    def normed(buf, row):
        def square(k, s):
            v = buf[k].astype(F32)
            return s + v * v
        total = lax.fori_loop(0, 8, square, jnp.zeros((T, 256), F32))
        factor = lax.rsqrt(jnp.sum(total, axis=1, keepdims=True) * (1.0 / 2048) + EPS)
        for k in range(8):
            cols = slice(k * 256, k * 256 + 256)
            XN[:, cols] = (buf[k].astype(F32) * factor * gains[row:row + 1, cols]).astype(BF)

    def norm_one():
        normed(X1, 0)

    def split_stats(s):
        high = s.astype(BF)
        low = (s - high.astype(F32)).astype(BF)
        return jnp.concatenate([high, low], axis=0)

    def mix():
        proj = jnp.dot(XN[...], M[...].reshape(2048, NM), preferred_element_type=F32)
        first, second = proj[:, :128], proj[:, 128:]
        u = first * pltpu.roll(first, 64, axis=1)
        place = lax.rem(lax.broadcasted_iota(jnp.int32, (T, 128), 0), LEN)
        lane = lax.broadcasted_iota(jnp.int32, (T, 128), 1)
        one = jnp.where(place >= 1, pltpu.roll(u, 1, axis=0), 0.0)
        two = jnp.where(place >= 2, pltpu.roll(u, 2, axis=0), 0.0)
        conv = small[2:3] * u + small[1:2] * one + small[0:1] * two
        mixed = jnp.where(lane >= 64, pltpu.roll(second, 64, axis=1) * conv, 0.0)
        sq = mixed * mixed
        high = sq.astype(BF)
        low = (sq - high.astype(F32)).astype(BF)
        ones = jnp.ones((16, 128), BF)
        nt = (((1,), (1,)), ((), ()))
        stat = (lax.dot_general(ones, high, nt, preferred_element_type=F32)
                + lax.dot_general(ones, low, nt, preferred_element_type=F32))[:8]
        scaled = (mixed * small[3:4]).astype(BF)
        for j in range(4):
            for mine in (False, True):
                core = c if mine else 1 - c
                w = M[lax.rem(x + j, 4), pl.ds(4 * core, 4), :, 128:].reshape(256, 128)
                part = lax.dot_general(w, scaled, nt, preferred_element_type=F32)
                if mine:
                    own32[j] = part
                else:
                    preo[j, :256] = part.astype(BF)
                    preo[j, 256:] = split_stats(stat)
        keep[0:8] = stat

    def mixsum():
        stat = keep[0:8] + prei[0, 256:264].astype(F32) + prei[0, 264:272].astype(F32)
        for j in (2, 1, 3):
            rxo[j - 1, :256] = (own32[j] + prei[j, :256].astype(F32)).astype(BF)
            rxo[j - 1, 256:] = split_stats(stat)
        own32[0] = own32[0] + prei[0, :256].astype(F32)
        keep[0:8] = stat

    def after():
        stat = keep[0:8]
        total = own32[0]
        for j in range(3):
            total = total + rxi[j, :256].astype(F32)
            stat = stat + rxi[j, 256:264].astype(F32) + rxi[j, 264:272].astype(F32)
        factor = lax.rsqrt(stat * (1.0 / 512) + EPS)[0:1]
        value = (res[...].astype(F32) + total * factor).astype(BF)
        X2[slot(0, c)] = value.astype(F32).T.astype(BF)
        out[...] = value

    def norm_two():
        normed(X2, 1)

    def hidden():
        for n in range(6):
            cols = slice(n * 256, min(n * 256 + 256, NG))
            w = G[:, :, :, cols].reshape(2048, cols.stop - cols.start)
            acc[:, cols] = jnp.dot(XN[...], w, preferred_element_type=F32) * gus[0:1, cols]
        lane = lax.broadcasted_iota(jnp.int32, (T, 128), 1)
        for n in range(6):
            even = acc[:, 256 * n:256 * n + 128]
            if n < 5:
                odd = acc[:, 256 * n + 128:256 * n + 256]
            else:
                odd = jnp.zeros((T, 128), F32)
            gate = jnp.where(lane < 64, even, odd)
            up = pltpu.roll(jnp.where(lane < 64, odd, even), 64, axis=1)
            hid[:, 128 * n:128 * n + 128] = (gate / (1.0 + jnp.exp(-gate)) * up).astype(BF)

    def down(j, core):
        w = D[lax.rem(x + j, 4), pl.ds(4 * core, 4)].reshape(256, ND)
        return lax.dot_general(w, hid[...], (((1,), (1,)), ((), ())), preferred_element_type=F32)

    def down_partner(j):
        qo[j] = down(j, 1 - c).astype(BF)

    def down_own():
        for j in range(4):
            own32[j] = down(j, c)

    def sum_for(j):
        ro[j - 1] = (own32[j] + qi[j].astype(F32)).astype(BF)

    def final():
        total = own32[0] + qi[0].astype(F32)
        for j in range(3):
            total = total + ri[j].astype(F32)
        out[...] = (out[...].astype(F32) + total).astype(BF)

    tasks = [
        ("norm1", all_x1, 2.0, norm_one),
        ("mix", ["norm1"] + all_m, 2.5, mix),
        ("mixsum", ["Q"], 0.7, mixsum),
        ("after", ["Rx+", "Rx-", "Rxx"], 0.7, after),
        ("norm2", all_x2, 2.0, norm_two),
        ("hidden", ["norm2"] + all_g, 4.0, hidden),
        ("down2", ["hidden"] + all_d, 0.3, lambda: down_partner(2)),
        ("down1", ["down2"], 0.3, lambda: down_partner(1)),
        ("down3", ["down1"], 0.3, lambda: down_partner(3)),
        ("down0", ["down3"], 0.3, lambda: down_partner(0)),
        ("own", ["down0"], 1.0, down_own),
        ("sum2", ["own", "S2"], 0.2, lambda: sum_for(2)),
        ("sum1", ["own", "S1"], 0.2, lambda: sum_for(1)),
        ("sum3", ["own", "S3"], 0.2, lambda: sum_for(3)),
        ("final", ["S0", "Ux+", "Ux-", "Uxx"], 0.5, final),
    ]
    order = plan_from(ev, tasks)
    for kind, item in order:
        if kind == "send":
            start(item)
        elif kind == "wait":
            arrive(item)
        else:
            item[3]()
    for e in ev:
        left(e)


def plan_from(events, tasks):
    for e in events:
        e.deps = [d for d in e.deps if not d.startswith("init")]
    return plan(events, tasks)


N_EVENTS = 12 + 40 + 18 + 7 + 1 + 3 + 7 + 4 + 3


def local(residual, mixer_gain, value_weight, value_scale, input_gate_weight, input_gate_scale,
          output_gate_weight, output_gate_scale, conv_taps, conv_gain, mixer_out_weight, mixer_out_scale,
          channel_gain, gate_weight, gate_scale, up_weight, up_scale, down_weight, down_scale):
    m = jnp.concatenate([value_weight, input_gate_weight, output_gate_weight,
                         mixer_out_weight.T * mixer_out_scale[:, None]], axis=1).astype(BF)
    even = (jnp.arange(11) % 2 == 0)[:, None]

    def laced(a, b):
        a = a.reshape(*a.shape[:-1], 11, 64)
        b = b.reshape(*b.shape[:-1], 11, 64)
        both = jnp.concatenate([jnp.where(even, a, b), jnp.where(even, b, a)], axis=-1)
        return both.reshape(*both.shape[:-2], NG)

    g = laced(gate_weight.astype(BF), up_weight.astype(BF))
    gus = jnp.broadcast_to(laced(gate_scale, up_scale)[None], (8, NG))
    d = jnp.pad((down_weight.T * down_scale[:, None]).astype(BF), ((0, 0), (0, ND - FFL)))
    factor = value_scale * input_gate_scale * output_gate_scale
    rows = jnp.concatenate([conv_taps * factor[None], conv_gain[None], jnp.zeros((4, 64), F32)], axis=0)
    small = jnp.concatenate([rows, rows], axis=1)
    gains = jnp.concatenate([mixer_gain[None], channel_gain[None], jnp.zeros((6, 2048), F32)], axis=0)
    hbm = pl.BlockSpec(memory_space=pl.ANY)
    vmem = pl.BlockSpec(memory_space=pltpu.VMEM)
    V = pltpu.VMEM
    return pl.pallas_call(
        functools.partial(kernel, n_events=N_EVENTS),
        out_shape=jax.ShapeDtypeStruct((256, T), BF),
        in_specs=[hbm] * 4 + [vmem] * 4,
        out_specs=vmem,
        scratch_shapes=[
            V((4, 8, 64, NM), BF), V((4, 8, 64, NG), BF), V((4, 8, 64, ND), BF),
            V((8, T, 256), BF), V((8, T, 256), BF), V((T, 2048), BF), V((T, NG), F32), V((T, ND), BF),
            V((8, T), F32), V((4, 256, T), F32),
            V((4, ST, T), BF), V((4, ST, T), BF), V((3, ST, T), BF), V((3, ST, T), BF),
            V((4, 256, T), BF), V((4, 256, T), BF), V((3, 256, T), BF), V((3, 256, T), BF),
            pltpu.SemaphoreType.DMA((N_EVENTS,)), pltpu.SemaphoreType.DMA((N_EVENTS,)),
            pltpu.SemaphoreType.DMA((4,)),
        ],
        compiler_params=pltpu.CompilerParams(collective_id=0, has_side_effects=True,
                                             vmem_limit_bytes=60 * 1024 * 1024),
        name="layer",
    )(m, g, d, residual.T, residual, small, gus, gains)


def solution(mesh):
    rf = ("rep", "fs")
    in_specs = (P("tp", rf), P(), P("fs", "tp"), P("tp"), P("fs", "tp"), P("tp"), P("fs", "tp"), P("tp"),
                P(None, "tp"), P("tp"), P("tp", "fs"), P("fs"), P(), P("fs", "tp"), P("tp"), P("fs", "tp"),
                P("tp"), P("tp", "fs"), P("fs"))
    return jax.shard_map(local, mesh=mesh, in_specs=in_specs, out_specs=P("tp", rf), check_vma=False)
```

time: 315 us -> 110 us (0.35)
  blocking collectives: 196 us -> 0 us
  Pallas kernels: 0 us -> 95.8 us
  starting transfers between devices: 52.5 us -> 0 us
  waiting for transfers between devices: 22 us -> 0 us
  between operations: 13.8 us -> 0.11 us
  matrix products: 13.6 us -> 0 us
  other arithmetic: 6.34 us -> 2.57 us
    all_gather x3 -> x0, blocking collectives: 159 us -> none  [the longest x1 77.3 us: sent_together(): lax.all_gather(both, axis, axis=dim, tiled=True)]
    pallas_call x0 -> x1, Pallas kernels: none -> 95.8 us  [local(): pl.pallas_call(functools.partial(kernel, n_events=N_EVENTS), out_shape=ja...]
    all_to_all x5 -> x0, starting transfers between devices: 52.5 us -> none  [the longest x4 36.6 us: copy_for_each(): lax.all_to_all(jnp.broadcast_to(value[None], (devices, *value.shape)), ax...]
    all_to_all x2 -> x0, blocking collectives: 36.8 us -> none  [the longest x1 18.4 us: copy_for_each(): lax.all_to_all(jnp.broadcast_to(value[None], (devices, *value.shape)), ax...]
    all_to_all x5 -> x0, waiting for transfers between devices: 21.9 us -> none  [the longest x4 15.4 us: copy_for_each(): lax.all_to_all(jnp.broadcast_to(value[None], (devices, *value.shape)), ax...]
    dot_general x6 -> x0, matrix products: 13.6 us -> none  [the longest x5 13.1 us: contract(): lax.dot_general(weight, rows, (((0,), (0,)), ((), ())), preferred_element...]
    unnamed x36 -> x41, local copies, waits for them, and re-layouts: 1.74 us -> 8.77 us
    convert_element_type x11 -> x1, other arithmetic: 3.7 us -> 0.08 us  [local(): (down_weight.T * down_scale[:, None]).astype(BF)]
  transfers between devices with their start and end apart: 7 -> 0, of which waited for: 3 -> 0; matrix products, arithmetic and copies ran while one was open for 5% -> 0% of each run, Pallas kernels for 0% -> 0%
where the time goes in v1:
time: 110 us
  Pallas kernels  95.8 us (87%)
  local copies, waits for them, and re-layouts  11.1 us (10%)
  other arithmetic  2.57 us (2%)
    pallas_call x1, Pallas kernels, local(): pl.pallas_call(functools.partial(kernel, n_events=N_EVENTS), out_shape=ja...  95.8 us
    unnamed x41, local copies, waits for them, and re-layouts  8.77 us

profile of v1, /device:TPU:1, one launch (start us, length us, event | category | flops | bytes accessed | tf_op | source)
XLA Modules:
  0.0 109.6 jit_solution(6810516699258954254)
XLA Ops:
  0.0 1.1 %copy.23 = bf16[64,704]{0,1:T(8,128)(2,1)S(1)} copy(f32[64,704]{1,0:T(8,128)} %param.32) | data formatting | bytes 270336 | tf_op args[13]
  1.1 0.2 copy.24
  1.3 0.1 broadcast_select_fusion.1
  1.4 0.1 pad_maximum_fusion
  1.5 0.0 copy-start.9
  1.5 0.8 copy.27.g_in
  2.4 0.1 reshape.32
  2.4 0.6 copy-done.10
  3.1 0.1 reshape.33
  3.1 0.1 broadcast_select_fusion.3
  3.2 0.1 maximum_bitcast_fusion
  3.3 0.6 broadcast_in_dim.57.gus
  3.9 0.0 copy-done.12
  3.9 0.1 fusion
  4.0 0.0 copy-start
  4.0 0.6 pad.4.d_in
  4.7 0.3 copy-done
  5.0 0.8 copy.26
  5.7 0.1 copy.22
  5.8 0.6 copy-done.13
  6.4 0.1 fusion.1
  6.5 0.7 copy-done.3
  7.2 0.8 copy-done.4
  7.9 0.8 copy-done.5
  8.7 0.7 pad_maximum_fusion.1.m_in
  9.4 0.1 pad.7.clone
  9.5 0.7 maximum_maximum_fusion.gains
  10.2 0.7 copy-done.11
  10.9 0.7 copy-done.14
  11.5 0.7 maximum_maximum_fusion.1.small
  12.2 95.8 %layer.1 = bf16[256,256]{1,0:T(8,128)(2,1)} custom-call(bf16[64,256]{1,0:T(8,128)(2,1)} %pad_maximum_fusion.1.m_in, bf16[64,1408]{1,0:T(8,128)(2,1)} %copy.27.g_in, bf16[64,768]{1,0:T(8,128)(2,1)} %pad.4.d_in, bf16[256,256]{1,0:T(8,128)(2,1)} %bitcast.16, bf16[256,256]{1,0:T(8,128)(2,1)} %res.1, f32[8,128]{1,0:T(8,128)} %maximum_maximum_fusion.1.small, ...), custom_call_target="tpu_custom_call" | custom-call | tf_op jit(solution)/shard_map/layer/pallas_call | solution.py:397
  108.0 1.6 %copy.29 = bf16[256,256]{1,0:T(8,128)(2,1)} copy(bf16[256,256]{1,0:T(8,128)(2,1)} %layer.1) | data formatting | bytes 262144
  (33 shorter events, 0.1 us)
Async XLA Ops:
  0.0 1.1 %copy-start.1 = (f32[64,704]{1,0:T(8,128)S(1)}, f32[64,704]{1,0:T(8,128)}, u32[]{:S(2)}) copy-start(f32[64,704]{1,0:T(8,128)} %param.34) | copy-start | bytes 540676
  1.5 0.9 copy-start.9
  1.5 2.4 %copy-start.2 = (f32[704,64]{0,1:T(8,128)S(1)}, f32[704,64]{0,1:T(8,128)}, u32[]{:S(2)}) copy-start(f32[704,64]{0,1:T(8,128)} %param.36) | copy-start | bytes 540676
  2.4 0.7 copy-start.10
  3.3 0.7 copy-start.12
  4.0 0.9 copy-start
  5.0 0.8 copy-start.6
  5.7 0.7 copy-start.13
  6.4 0.8 copy-start.3
  7.1 0.8 copy-start.4
  7.9 0.8 copy-start.5
  8.7 0.8 copy-start.7
  8.7 0.8 copy-start.8
  9.5 0.7 copy-start.15
  9.5 0.7 copy-start.16
  9.5 0.7 copy-start.17
  10.2 0.7 copy-start.11
  10.9 0.7 copy-start.14

commit v2 on v1

v2 whole, which is shorter than its diff:
```python
import functools

import jax
import jax.numpy as jnp
from jax import lax
from jax.experimental import pallas as pl
from jax.experimental.pallas import tpu as pltpu
from jax.sharding import PartitionSpec as P

MESH = pl.DeviceIdType.MESH
F32 = jnp.float32
BF = jnp.bfloat16
EPS = 1e-06
LEN = 128
T = 256
NM, G1L, G2L, DL = 256, 1024, 384, 384
FFL = 704
ST = 272


class Event:
    def __init__(self, name, link, size, deps, put, got):
        self.name, self.link, self.size, self.deps = name, link, size, deps
        self.put, self.got = put, got


RATE = {"p": 300.0, "xx": 23.0}
LAT = {"p": 1.0, "xx": 2.6}


def plan(events, tasks):
    done, order, sent, flights = set(), [], set(), []
    free = {}
    now = 0.0

    def launch():
        for e in events:
            if e.name not in sent and all(d in done for d in e.deps):
                sent.add(e.name)
                start = max(now, free.get(e.link, 0.0))
                end = start + e.size / (RATE.get(e.link, 46.0) * 1e3)
                free[e.link] = end
                flights.append((end + LAT.get(e.link, 1.8), e))
                order.append(("send", e))

    launch()
    left = list(tasks)
    while flights or left:
        ready = [t for t in left if all(d in done for d in t[1])]
        landed = [f for f in flights if f[0] <= now]
        if landed:
            f = min(landed, key=lambda v: v[0])
        elif ready:
            t = ready[0]
            left.remove(t)
            order.append(("run", t))
            now += t[2]
            done.add(t[0])
            launch()
            continue
        else:
            f = min(flights, key=lambda v: v[0])
            now = f[0]
        flights.remove(f)
        order.append(("wait", f[1]))
        done.add(f[1].name)
        launch()
    return order


def weight_events(M, G1, G2, D1, D2, W):
    ev = []

    def add(name, link, size, deps, ref):
        ev.append(Event(name, link, size, deps, lambda: ref(*W.shift[link]), lambda: ref(0, 0)))

    def along_z(tag, buf, width, b, have):
        size = 64 * width * 2
        for sign, link in ((-1, "z+"), (1, "z-")):
            add(f"{tag}{link}1", link, size, have, lambda dz, dy, s=sign: buf.at[W.zl(s + dz), W.yy(b + dy)])
        for sign, link, lo in ((-1, "z+", 0), (1, "z-", 32)):
            add(f"{tag}{link}2", link, size // 2, [f"{tag}{link}1"],
                lambda dz, dy, s=sign, lo=lo: buf.at[W.zl(2 * s + dz), W.yy(b + dy), pl.ds(lo, 32)])
        return [f"{tag}z+1", f"{tag}z-1", f"{tag}z+2", f"{tag}z-2"]

    def columns_along_y(tag, buf, width, first):
        names = []
        for s in (1, 2, 3, 4):
            for sign, link, lo in ((-1, "y+", 0), (1, "y-", 2)):
                n, at = (4, 0) if s < 4 else (2, lo)
                add(f"{tag}{link}{s}", link, n * 64 * width * 2, first if s == 1 else [f"{tag}{link}{s - 1}"],
                    lambda dz, dy, s=s, sign=sign, at=at, n=n: buf.at[pl.ds(at, n), W.yy(sign * s + dy)])
                names.append(f"{tag}{link}{s}")
        return names

    def own_along_y(tag, buf, width, first):
        for s in (1, 2, 3, 4):
            for sign, link, lo in ((-1, "y+", 0), (1, "y-", 32)):
                n, at = (64, 0) if s < 4 else (32, lo)
                add(f"{tag}{link}{s}", link, n * width * 2, first if s == 1 else [f"{tag}{link}{s - 1}"],
                    lambda dz, dy, s=s, sign=sign, at=at, n=n: buf.at[W.zl(dz), W.yy(sign * s + dy), pl.ds(at, n)])

    def behind(tag, b):
        if b == 0:
            return []
        if b == 4:
            return [f"{tag}y+4", f"{tag}y-4"]
        return [f"{tag}y+{-b}"] if b < 0 else [f"{tag}y-{b}"]

    mz = along_z("M", M, NM, 0, [])
    all_m = mz + columns_along_y("M", M, NM, mz)
    own_along_y("G", G1, G1L, [])
    g2z = along_z("H", G2, G2L, 0, [])
    all_g = []
    for b in (0, -1, 1, -2, 2, -3, 3, 4):
        all_g += behind("G", b) + along_z(f"G{b}", G1, G1L, b, behind("G", b))
    d1z = along_z("D", D1, DL, 0, [])
    own_along_y("E", D2, DL, ["Gy+2", "Gy-2"])
    all_h = g2z + columns_along_y("H", G2, G2L, g2z + ["My+2", "My-2"])
    d1y = columns_along_y("D", D1, DL, d1z + ["Hy+3", "Hy-3"])
    of_y = {0: list(d1z)}
    for s in (1, 2, 3):
        of_y[-s] = [f"Dy+{s}"]
        of_y[s] = [f"Dy-{s}"]
    of_y[4] = ["Dy+4", "Dy-4"]
    for b in (2, -2, 1, -1, -3, 3, 0, 4):
        late = ["G3z+1", "G3z-1"]
        of_y[b] = of_y[b] + behind("E", b) + along_z(f"E{b}", D2, DL, b, behind("E", b) + late)
    return ev, all_m, all_g, all_h, of_y


class Where:
    pass


def kernel(res_in, mgain_in, cgain_in, v_in, i_in, o_in, w_in, g_in, u_in, d_in,
           vs_in, is_in, os_in, taps_in, cg_in, ms_in, gs_in, us_in, ds_in, out,
           M, G1, G2, D1, D2, X1, X2, XN, hid, keep, own32, preo, prei, rxo, rxi, qo, qi, ro, ri,
           res, mgain, cgain, vw, iw, ow, mw, gw, uw, dw, vs, ivs, ovs, taps, cg, ms, gs, us, ds, small,
           send_sem, recv_sem, loc_sem, n_events):
    rep, fs, tp = lax.axis_index("rep"), lax.axis_index("fs"), lax.axis_index("tp")
    y, zl = lax.rem(fs, 8), lax.div(fs, 8)
    x, c = lax.div(tp, 2), lax.rem(tp, 2)
    z = rep * 4 + zl

    def y_at(d):
        return {"fs": zl * 8 + lax.rem(y + d + 8, 8)}

    def z_at(d):
        zz = lax.rem(z + d + 8, 8)
        return {"rep": lax.div(zz, 4), "fs": lax.rem(zz, 4) * 8 + y}

    def x_at(d):
        return {"tp": lax.rem(x + d + 4, 4) * 2 + c}

    partner = {"tp": x * 2 + 1 - c}
    target = {"y+": y_at(1), "y-": y_at(-1), "z+": z_at(1), "z-": z_at(-1),
              "x+": x_at(1), "x-": x_at(-1), "xx": x_at(2), "p": partner}

    W = Where()
    W.shift = {"y+": (0, 1), "y-": (0, -1), "z+": (1, 0), "z-": (-1, 0)}
    W.zl = lambda d: lax.rem(zl + d + 8, 4)
    W.yy = lambda d: lax.rem(y + d + 16, 8)

    ev, all_m, all_g, all_h, of_y = weight_events(M, G1, G2, D1, D2, W)
    pos = {"x+": -1, "x-": 1, "xx": 2}

    def slot(d, core):
        return lax.rem(x + d + 4, 4) * 2 + core

    def spread(tag, buf, first):
        names = []
        for link in ("x+", "x-", "xx"):
            ev.append(Event(f"{tag}{link}", link, T * 256 * 2, [first] if first else [],
                            lambda: buf.at[slot(0, c)], lambda link=link: buf.at[slot(pos[link], c)]))
            names.append(f"{tag}{link}")
        ev.append(Event(f"{tag}p", "p", T * 256 * 2, [first] if first else [],
                        lambda: buf.at[slot(0, c)], lambda: buf.at[slot(0, 1 - c)]))
        names.append(f"{tag}p")
        for link in ("x+", "x-", "xx"):
            ev.append(Event(f"{tag}p{link}", "p", T * 256 * 2, [f"{tag}{link}"],
                            lambda link=link: buf.at[slot(pos[link], c)],
                            lambda link=link: buf.at[slot(pos[link], 1 - c)]))
            names.append(f"{tag}p{link}")
        return names

    all_x1 = spread("X1", X1, None)
    hop = {"x+": 1, "x-": 3, "xx": 2}
    ev.append(Event("Q", "p", 4 * ST * T * 2, ["mix"], lambda: preo, lambda: prei))
    for link, j in hop.items():
        ev.append(Event(f"R{link}", link, ST * T * 2, ["mixsum"],
                        lambda j=j: rxo.at[j - 1], lambda j=j: rxi.at[j - 1]))
    all_x2 = spread("X2", X2, "after")
    for g in range(4):
        ev.append(Event(f"S{g}", "p", 256 * T * 2, [f"down{g}"], lambda g=g: qo.at[g], lambda g=g: qi.at[g]))
        for link, j in hop.items():
            ev.append(Event(f"U{g}{link}", link, 64 * T * 2, [f"sum{g}"],
                            lambda j=j, g=g: ro.at[g, j - 1], lambda j=j, g=g: ri.at[g, j - 1]))
    assert len(ev) == n_events, len(ev)
    index = {e.name: i for i, e in enumerate(ev)}

    barrier = pltpu.get_barrier_semaphore()
    for dev in target.values():
        pl.semaphore_signal(barrier, inc=1, device_id=dev, device_id_type=MESH)

    ins = [(res_in, res), (v_in, vw), (i_in, iw), (o_in, ow), (w_in, mw), (ms_in, ms), (g_in, gw), (u_in, uw),
           (d_in, dw), (ds_in, ds), (mgain_in, mgain), (cgain_in, cgain), (vs_in, vs), (is_in, ivs), (os_in, ovs),
           (taps_in, taps), (cg_in, cg), (gs_in, gs), (us_in, us)]
    copies = [pltpu.make_async_copy(src, dst, loc_sem.at[i]) for i, (src, dst) in enumerate(ins)]
    for copy in copies:
        copy.start()
    for copy in copies:
        copy.wait()
    half = lax.broadcasted_iota(jnp.int32, (64, 128), 1) < 64
    X1[slot(0, c)] = res[...].astype(F32).T.astype(BF)
    own = (zl, y)
    M[(*own, slice(None), slice(0, 128))] = jnp.concatenate([vw[...], iw[...]], axis=1).astype(BF)
    turned = (mw[...] * ms[...]).T
    M[(*own, slice(None), slice(128, 256))] = jnp.concatenate([ow[...], turned], axis=1).astype(BF)
    for t in range(6):
        if t < 5:
            gate, up = gw[:, 128 * t:128 * t + 128], uw[:, 128 * t:128 * t + 128]
        else:
            gate = jnp.concatenate([gw[:, 640:704]] * 2, axis=1)
            up = jnp.concatenate([uw[:, 640:704]] * 2, axis=1)
        turn = pltpu.roll(up, 64, axis=1)
        pair = [jnp.where(half, gate, turn).astype(BF), jnp.where(half, turn, gate).astype(BF)]
        for k in range(2 if t < 5 else 1):
            n = 2 * t + k
            if n < 8:
                G1[(*own, slice(None), slice(128 * n, 128 * n + 128))] = pair[k]
            else:
                n -= 8
                G2[(*own, slice(None), slice(128 * n, 128 * n + 128))] = pair[k]
    D1[own] = (dw[0:384] * ds[...]).T.astype(BF)
    D2[(*own, slice(None), slice(0, 256))] = (dw[384:640] * ds[...]).T.astype(BF)
    tail = (dw[640:704] * ds[...]).T
    D2[(*own, slice(None), slice(256, 384))] = jnp.concatenate([tail, jnp.zeros((64, 64), F32)], axis=1).astype(BF)
    row = vs[...] * ivs[...] * ovs[...]
    for k in range(3):
        line = taps[k:k + 1] * row
        small[k:k + 1] = jnp.concatenate([line, line], axis=1)
    small[3:4] = jnp.concatenate([cg[...], cg[...]], axis=1)
    pl.semaphore_wait(barrier, 8)

    def start(e):
        i = index[e.name]
        ref = e.put()
        pltpu.make_async_remote_copy(src_ref=ref, dst_ref=ref if e.link[0] in "yz" or e.name[:1] == "X" else e.got(),
                                     send_sem=send_sem.at[i], recv_sem=recv_sem.at[i],
                                     device_id=target[e.link], device_id_type=MESH).start()

    def arrive(e):
        i = index[e.name]
        ref = e.got()
        pltpu.make_async_remote_copy(src_ref=ref, dst_ref=ref, send_sem=send_sem.at[i], recv_sem=recv_sem.at[i],
                                     device_id=target[e.link], device_id_type=MESH).wait_recv()

    def left(e):
        i = index[e.name]
        ref = e.put()
        pltpu.make_async_remote_copy(src_ref=ref, dst_ref=ref, send_sem=send_sem.at[i], recv_sem=recv_sem.at[i],
                                     device_id=target[e.link], device_id_type=MESH).wait_send()

    def normed(buf, gain):
        def square(k, s):
            v = buf[k].astype(F32)
            return s + v * v
        total = lax.fori_loop(0, 8, square, jnp.zeros((T, 256), F32))
        factor = lax.rsqrt(jnp.sum(total, axis=1, keepdims=True) * (1.0 / 2048) + EPS)
        for k in range(8):
            cols = slice(k * 256, k * 256 + 256)
            XN[:, cols] = (buf[k].astype(F32) * factor * gain[0:1, cols]).astype(BF)

    def norm_one():
        normed(X1, mgain)

    def split_stats(s):
        high = s.astype(BF)
        low = (s - high.astype(F32)).astype(BF)
        return jnp.concatenate([high, low], axis=0)

    def mix():
        proj = jnp.dot(XN[...], M[...].reshape(2048, NM), preferred_element_type=F32)
        first, second = proj[:, :128], proj[:, 128:]
        u = first * pltpu.roll(first, 64, axis=1)
        place = lax.rem(lax.broadcasted_iota(jnp.int32, (T, 128), 0), LEN)
        lane = lax.broadcasted_iota(jnp.int32, (T, 128), 1)
        one = jnp.where(place >= 1, pltpu.roll(u, 1, axis=0), 0.0)
        two = jnp.where(place >= 2, pltpu.roll(u, 2, axis=0), 0.0)
        conv = small[2:3] * u + small[1:2] * one + small[0:1] * two
        mixed = jnp.where(lane >= 64, pltpu.roll(second, 64, axis=1) * conv, 0.0)
        sq = mixed * mixed
        high = sq.astype(BF)
        low = (sq - high.astype(F32)).astype(BF)
        ones = jnp.ones((16, 128), BF)
        nt = (((1,), (1,)), ((), ()))
        stat = (lax.dot_general(ones, high, nt, preferred_element_type=F32)
                + lax.dot_general(ones, low, nt, preferred_element_type=F32))[:8]
        scaled = (mixed * small[3:4]).astype(BF)
        for j in range(4):
            for mine in (False, True):
                core = c if mine else 1 - c
                w = M[lax.rem(x + j, 4), pl.ds(4 * core, 4), :, 128:].reshape(256, 128)
                part = lax.dot_general(w, scaled, nt, preferred_element_type=F32)
                if mine:
                    own32[j] = part
                else:
                    preo[j, :256] = part.astype(BF)
                    preo[j, 256:] = split_stats(stat)
        keep[0:8] = stat

    def mixsum():
        stat = keep[0:8] + prei[0, 256:264].astype(F32) + prei[0, 264:272].astype(F32)
        for j in (2, 1, 3):
            rxo[j - 1, :256] = (own32[j] + prei[j, :256].astype(F32)).astype(BF)
            rxo[j - 1, 256:] = split_stats(stat)
        own32[0] = own32[0] + prei[0, :256].astype(F32)
        keep[0:8] = stat

    def after():
        stat = keep[0:8]
        total = own32[0]
        for j in range(3):
            total = total + rxi[j, :256].astype(F32)
            stat = stat + rxi[j, 256:264].astype(F32) + rxi[j, 264:272].astype(F32)
        factor = lax.rsqrt(stat * (1.0 / 512) + EPS)[0:1]
        value = (res[...].astype(F32) + total * factor).astype(BF)
        X2[slot(0, c)] = value.astype(F32).T.astype(BF)
        out[...] = value

    def norm_two():
        normed(X2, cgain)

    lane = lax.broadcasted_iota(jnp.int32, (T, 128), 1)

    def hidden_tiles(w, first, tiles):
        z = jnp.dot(XN[...], w, preferred_element_type=F32)
        for k in range(0, tiles, 2):
            n = (first + k) // 2
            even = z[:, 128 * k:128 * k + 128]
            if k + 1 < tiles:
                odd = z[:, 128 * k + 128:128 * k + 256]
                gsc, usc = gs[0:1, 128 * n:128 * n + 128], us[0:1, 128 * n:128 * n + 128]
            else:
                odd = jnp.zeros((T, 128), F32)
                gsc = jnp.concatenate([gs[0:1, 640:704]] * 2, axis=1)
                usc = jnp.concatenate([us[0:1, 640:704]] * 2, axis=1)
            gate = jnp.where(lane < 64, even, odd) * gsc
            up = pltpu.roll(jnp.where(lane < 64, odd, even), 64, axis=1) * usc
            hid[:, 128 * n:128 * n + 128] = (gate / (1.0 + jnp.exp(-gate)) * up).astype(BF)

    def hidden_one():
        for n in range(4):
            hidden_tiles(G1[:, :, :, n * 256:n * 256 + 256].reshape(2048, 256), 2 * n, 2)

    def hidden_two():
        hidden_tiles(G2[:, :, :, 0:256].reshape(2048, 256), 8, 2)
        hidden_tiles(G2[:, :, :, 256:384].reshape(2048, 128), 10, 1)

    def down(g, core):
        at = lax.rem(y + g, 4) + 4 * core
        nt = (((1,), (1,)), ((), ()))
        p = lax.dot_general(D1[:, at].reshape(256, DL), hid[:, :DL], nt, preferred_element_type=F32)
        q = lax.dot_general(D2[:, at].reshape(256, DL), hid[:, DL:], nt, preferred_element_type=F32)
        return (p + q).reshape(4, 64, T)

    def down_partner(g):
        qo[g] = down(g, 1 - c).astype(BF)

    def down_own(g):
        own32[g] = down(g, c).reshape(256, T)

    def sum_for(g):
        for j in (2, 1, 3):
            x_to = lax.rem(x + j, 4)
            ro[g, j - 1] = (own32[g, pl.ds(pl.multiple_of(x_to * 64, 64), 64)] + qi[g, x_to].astype(F32)).astype(BF)

    def final(g):
        rows = pl.ds(pl.multiple_of(lax.rem(y + g, 4) * 64, 64), 64)
        total = own32[g, pl.ds(pl.multiple_of(x * 64, 64), 64)] + qi[g, x].astype(F32)
        for j in range(3):
            total = total + ri[g, j].astype(F32)
        out[rows] = (out[rows].astype(F32) + total).astype(BF)

    tasks = [
        ("norm1", all_x1, 0.8, norm_one),
        ("mix", ["norm1"] + all_m, 1.5, mix),
        ("mixsum", ["Q"], 0.5, mixsum),
        ("after", ["Rx+", "Rx-", "Rxx"], 0.5, after),
        ("norm2", all_x2, 0.8, norm_two),
        ("hidden1", ["norm2"] + all_g, 1.4, hidden_one),
        ("hidden2", ["norm2"] + all_h, 0.6, hidden_two),
    ]
    for g in (2, 1, 3, 0):
        need = of_y[g] + (of_y[g - 4] if g else of_y[4])
        tasks.append((f"down{g}", ["hidden1", "hidden2"] + need, 0.4, lambda g=g: down_partner(g)))
        tasks.append((f"own{g}", [f"down{g}"], 0.4, lambda g=g: down_own(g)))
        tasks.append((f"sum{g}", [f"own{g}", f"S{g}"], 0.2, lambda g=g: sum_for(g)))
    for g in (2, 1, 3, 0):
        tasks.append((f"final{g}", [f"U{g}x+", f"U{g}x-", f"U{g}xx"], 0.1, lambda g=g: final(g)))
    order = plan(ev, tasks)
    for kind, item in order:
        if kind == "send":
            start(item)
        elif kind == "wait":
            arrive(item)
        else:
            item[3]()
    for e in ev:
        left(e)


N_EVENTS = 12 + 40 + 12 + 12 + 40 + 7 + 1 + 3 + 7 + 4 + 12


def local(residual, mixer_gain, value_weight, value_scale, input_gate_weight, input_gate_scale,
          output_gate_weight, output_gate_scale, conv_taps, conv_gain, mixer_out_weight, mixer_out_scale,
          channel_gain, gate_weight, gate_scale, up_weight, up_scale, down_weight, down_scale):
    def line(a):
        return a.reshape(1, -1)

    hbm = pl.BlockSpec(memory_space=pl.ANY)
    vmem = pl.BlockSpec(memory_space=pltpu.VMEM)
    V = pltpu.VMEM
    return pl.pallas_call(
        functools.partial(kernel, n_events=N_EVENTS),
        out_shape=jax.ShapeDtypeStruct((256, T), BF),
        in_specs=[hbm] * 19,
        out_specs=vmem,
        scratch_shapes=[
            V((4, 8, 64, NM), BF), V((4, 8, 64, G1L), BF), V((4, 8, 64, G2L), BF),
            V((4, 8, 64, DL), BF), V((4, 8, 64, DL), BF),
            V((8, T, 256), BF), V((8, T, 256), BF), V((T, 2048), BF), V((T, 2 * DL), BF),
            V((8, T), F32), V((4, 256, T), F32),
            V((4, ST, T), BF), V((4, ST, T), BF), V((3, ST, T), BF), V((3, ST, T), BF),
            V((4, 4, 64, T), BF), V((4, 4, 64, T), BF), V((4, 3, 64, T), BF), V((4, 3, 64, T), BF),
            V((256, T), BF), V((1, 2048), F32), V((1, 2048), F32), V((64, 64), F32), V((64, 64), F32),
            V((64, 64), F32), V((64, 64), F32), V((64, FFL), F32), V((64, FFL), F32), V((FFL, 64), F32),
            V((1, 64), F32), V((1, 64), F32), V((1, 64), F32), V((3, 64), F32), V((1, 64), F32), V((1, 64), F32),
            V((1, FFL), F32), V((1, FFL), F32), V((1, 64), F32), V((8, 128), F32),
            pltpu.SemaphoreType.DMA((N_EVENTS,)), pltpu.SemaphoreType.DMA((N_EVENTS,)),
            pltpu.SemaphoreType.DMA((19,)),
        ],
        compiler_params=pltpu.CompilerParams(collective_id=0, has_side_effects=True,
                                             vmem_limit_bytes=60 * 1024 * 1024),
        name="layer",
    )(residual, line(mixer_gain), line(channel_gain), value_weight, input_gate_weight, output_gate_weight,
      mixer_out_weight, gate_weight, up_weight, down_weight, line(value_scale), line(input_gate_scale),
      line(output_gate_scale), conv_taps, line(conv_gain), line(mixer_out_scale), line(gate_scale),
      line(up_scale), line(down_scale))


def solution(mesh):
    rf = ("rep", "fs")
    in_specs = (P("tp", rf), P(), P("fs", "tp"), P("tp"), P("fs", "tp"), P("tp"), P("fs", "tp"), P("tp"),
                P(None, "tp"), P("tp"), P("tp", "fs"), P("fs"), P(), P("fs", "tp"), P("tp"), P("fs", "tp"),
                P("tp"), P("tp", "fs"), P("fs"))
    return jax.shard_map(local, mesh=mesh, in_specs=in_specs, out_specs=P("tp", rf), check_vma=False)
```

time: 110 us -> 95.8 us (0.87)
  local copies, waits for them, and re-layouts: 11.1 us -> 5.26 us
  Pallas kernels: 95.8 us -> 90.4 us
  other arithmetic: 2.57 us -> 0 us
    pallas_call x1, Pallas kernels: 95.8 us -> 90.4 us  [local(): pl.pallas_call(functools.partial(kernel, n_events=N_EVENTS), out_shape=ja...]
    unnamed x41 -> x6, local copies, waits for them, and re-layouts: 8.77 us -> 4.08 us
    concatenate x4 -> x0, other arithmetic: 2.14 us -> none  [the longest x1 0.7 us: local(): jnp.concatenate([mixer_gain[None], channel_gain[None], jnp.zeros((6, 2048...]
where the time goes in v2:
time: 95.8 us; the launch traced here: 95.6 us
  Pallas kernels  90.4 us (94%)
  local copies, waits for them, and re-layouts  5.26 us (5%)
    pallas_call x1, Pallas kernels, local(): pl.pallas_call(functools.partial(kernel, n_events=N_EVENTS), out_shape=ja...  90.4 us
    unnamed x6, local copies, waits for them, and re-layouts  4.08 us

profile of v2, /device:TPU:1, one launch (start us, length us, event | category | flops | bytes accessed | tf_op | source)
XLA Modules:
  0.0 95.6 jit_solution(12678931468025694804)
XLA Ops:
  0.0 0.0 copy-start
  0.0 0.0 copy-start.1
  0.0 0.7 copy-done
  0.7 0.6 reshape.37.gs_in
  1.3 0.0 copy-done.1
  1.3 0.6 reshape.38.us_in
  1.9 1.8 %copy.20.d_in = f32[704,64]{1,0:T(8,128)} copy(f32[704,64]{0,1:T(8,128)} %param.36) | data formatting | bytes 360448 | tf_op args[17]
  3.7 90.4 %layer.1 = bf16[256,256]{1,0:T(8,128)(2,1)} custom-call(bf16[256,256]{1,0:T(8,128)(2,1)} %res_in.1, f32[1,2048]{1,0:T(1,128)} %bitcast.8, f32[1,2048]{1,0:T(1,128)} %bitcast.9, f32[64,64]{1,0:T(8,128)} %v_in.1, f32[64,64]{1,0:T(8,128)} %i_in.1, f32[64,64]{1,0:T(8,128)} %o_in.1, f32[64,64]{1,0:T(8,128)} %w_in.1, f32[64,704]{1,0:T(8,128)} %g_in.1, ...), custom_call_target="tpu_custom_call" | custom-call | tf_op jit(solution)/shard_map/layer/pallas_call | solution.py:426
  94.1 1.6 %copy.22 = bf16[256,256]{1,0:T(8,128)(2,1)} copy(bf16[256,256]{1,0:T(8,128)(2,1)} %layer.1) | data formatting | bytes 262144
Async XLA Ops:
  0.0 0.7 copy-start
  0.0 1.3 %copy-start.1 = (f32[704]{0:T(1024)S(1)}, f32[704]{0:T(1024)}, u32[]{:S(2)}) copy-start(f32[704]{0:T(1024)} %param.35) | copy-start | bytes 8452

commit v3 on v2

--- a/solution.py
+++ b/solution.py
@@ -13,7 +13,7 @@
 EPS = 1e-06
 LEN = 128
 T = 256
-NM, G1L, G2L, DL = 256, 1024, 384, 384
+NM, G1L, G2L, D1L, D2L = 256, 1024, 384, 256, 512
 FFL = 704
 ST = 272
 
@@ -24,12 +24,15 @@
         self.put, self.got = put, got
 
 
-RATE = {"p": 300.0, "xx": 23.0}
-LAT = {"p": 1.0, "xx": 2.6}
+RATE = {"p": 100.0, "xx": 28.0, "x+": 60.0, "x-": 60.0}
+LAT = {"p": 1.5, "xx": 2.6}
 
 
 def plan(events, tasks):
     done, order, sent, flights = set(), [], set(), []
+    passed_on = {d for e in events for d in e.deps}
+    by_name = {e.name: e for e in events}
+    waited = set()
     free = {}
     now = 0.0
 
@@ -53,6 +56,10 @@
         elif ready:
             t = ready[0]
             left.remove(t)
+            for d in t[1]:
+                if d in by_name and d not in waited:
+                    waited.add(d)
+                    order.append(("wait", by_name[d]))
             order.append(("run", t))
             now += t[2]
             done.add(t[0])
@@ -62,7 +69,9 @@
             f = min(flights, key=lambda v: v[0])
             now = f[0]
         flights.remove(f)
-        order.append(("wait", f[1]))
+        if f[1].name in passed_on:
+            waited.add(f[1].name)
+            order.append(("wait", f[1]))
         done.add(f[1].name)
         launch()
     return order
@@ -83,21 +92,27 @@
                 lambda dz, dy, s=sign, lo=lo: buf.at[W.zl(2 * s + dz), W.yy(b + dy), pl.ds(lo, 32)])
         return [f"{tag}z+1", f"{tag}z-1", f"{tag}z+2", f"{tag}z-2"]
 
+    def gate(tag, s, link):
+        other = GATE.get(f"{tag}{s}")
+        return [f"{other[0]}{link}{other[1]}"] if other else []
+
     def columns_along_y(tag, buf, width, first):
         names = []
         for s in (1, 2, 3, 4):
             for sign, link, lo in ((-1, "y+", 0), (1, "y-", 2)):
                 n, at = (4, 0) if s < 4 else (2, lo)
-                add(f"{tag}{link}{s}", link, n * 64 * width * 2, first if s == 1 else [f"{tag}{link}{s - 1}"],
+                add(f"{tag}{link}{s}", link, n * 64 * width * 2,
+                    (first if s == 1 else [f"{tag}{link}{s - 1}"]) + gate(tag, s, link),
                     lambda dz, dy, s=s, sign=sign, at=at, n=n: buf.at[pl.ds(at, n), W.yy(sign * s + dy)])
                 names.append(f"{tag}{link}{s}")
         return names
 
-    def own_along_y(tag, buf, width, first):
+    def own_along_y(tag, buf, width):
         for s in (1, 2, 3, 4):
             for sign, link, lo in ((-1, "y+", 0), (1, "y-", 32)):
                 n, at = (64, 0) if s < 4 else (32, lo)
-                add(f"{tag}{link}{s}", link, n * width * 2, first if s == 1 else [f"{tag}{link}{s - 1}"],
+                add(f"{tag}{link}{s}", link, n * width * 2,
+                    ([] if s == 1 else [f"{tag}{link}{s - 1}"]) + gate(tag, s, link),
                     lambda dz, dy, s=s, sign=sign, at=at, n=n: buf.at[W.zl(dz), W.yy(sign * s + dy), pl.ds(at, n)])
 
     def behind(tag, b):
@@ -107,26 +122,47 @@
             return [f"{tag}y+4", f"{tag}y-4"]
         return [f"{tag}y+{-b}"] if b < 0 else [f"{tag}y-{b}"]
 
-    mz = along_z("M", M, NM, 0, [])
-    all_m = mz + columns_along_y("M", M, NM, mz)
-    own_along_y("G", G1, G1L, [])
-    g2z = along_z("H", G2, G2L, 0, [])
-    all_g = []
-    for b in (0, -1, 1, -2, 2, -3, 3, 4):
-        all_g += behind("G", b) + along_z(f"G{b}", G1, G1L, b, behind("G", b))
-    d1z = along_z("D", D1, DL, 0, [])
-    own_along_y("E", D2, DL, ["Gy+2", "Gy-2"])
-    all_h = g2z + columns_along_y("H", G2, G2L, g2z + ["My+2", "My-2"])
-    d1y = columns_along_y("D", D1, DL, d1z + ["Hy+3", "Hy-3"])
-    of_y = {0: list(d1z)}
+    def z_names(tag):
+        return [f"{tag}z+1", f"{tag}z-1", f"{tag}z+2", f"{tag}z-2"]
+
+    need = {}
+    of_y = {0: z_names("D"), 4: ["Dy+4", "Dy-4"]}
     for s in (1, 2, 3):
         of_y[-s] = [f"Dy+{s}"]
         of_y[s] = [f"Dy-{s}"]
-    of_y[4] = ["Dy+4", "Dy-4"]
-    for b in (2, -2, 1, -1, -3, 3, 0, 4):
-        late = ["G3z+1", "G3z-1"]
-        of_y[b] = of_y[b] + behind("E", b) + along_z(f"E{b}", D2, DL, b, behind("E", b) + late)
-    return ev, all_m, all_g, all_h, of_y
+    for part in FIRST:
+        if part == "M":
+            need["M"] = along_z("M", M, NM, 0, []) + columns_along_y("M", M, NM, z_names("M"))
+        elif part == "G":
+            own_along_y("G", G1, G1L)
+        elif part == "E":
+            own_along_y("E", D2, D2L)
+        elif part == "Hz":
+            along_z("H", G2, G2L, 0, [])
+        elif part == "Dz":
+            along_z("D", D1, D1L, 0, [])
+        elif part == "H":
+            need["H"] = z_names("H") + columns_along_y("H", G2, G2L, z_names("H"))
+        elif part == "D":
+            columns_along_y("D", D1, D1L, z_names("D"))
+        elif part == "Gz":
+            need["G"] = []
+            for b in (0, -1, 1, -2, 2, -3, 3, 4):
+                need["G"] += behind("G", b) + along_z(f"G{b}", G1, G1L, b, behind("G", b))
+        else:
+            for b in LAST:
+                of_y[b] = of_y[b] + behind("E", b) + along_z(f"E{b}", D2, D2L, b, behind("E", b) + z_names(HOLD)[:2])
+    return ev, need["M"], need["G"], need["H"], of_y
+
+
+FIRST = ("Hz", "M", "H", "E", "Gz", "Dz", "Ez", "G", "D")
+LAST = (2, -2, 3, -1, -3, 4, 1, 0)
+HOLD = "G4"
+GROUPS = (2, 1, 0, 3)
+GATE = {
+    "H1": "M3", "E2": "G4", "D1": "H1", "M2": "E1", "G3": "G2", "H3": "E2", "D2": "G3", "E3": "E1", "D3":
+    "D1", "G4": "G3", "H2": "M4",
+}
 
 
 class Where:
@@ -135,7 +171,7 @@
 
 def kernel(res_in, mgain_in, cgain_in, v_in, i_in, o_in, w_in, g_in, u_in, d_in,
            vs_in, is_in, os_in, taps_in, cg_in, ms_in, gs_in, us_in, ds_in, out,
-           M, G1, G2, D1, D2, X1, X2, XN, hid, keep, own32, preo, prei, rxo, rxi, qo, qi, ro, ri,
+           M, G1, G2, D1, D2, X1, X2, XN, hid, keep, mixed_to, own32, preo, prei, rxo, rxi, qo, qi, ro, ri,
            res, mgain, cgain, vw, iw, ow, mw, gw, uw, dw, vs, ivs, ovs, taps, cg, ms, gs, us, ds, small,
            send_sem, recv_sem, loc_sem, n_events):
     rep, fs, tp = lax.axis_index("rep"), lax.axis_index("fs"), lax.axis_index("tp")
@@ -186,9 +222,10 @@
 
     all_x1 = spread("X1", X1, None)
     hop = {"x+": 1, "x-": 3, "xx": 2}
-    ev.append(Event("Q", "p", 4 * ST * T * 2, ["mix"], lambda: preo, lambda: prei))
-    for link, j in hop.items():
-        ev.append(Event(f"R{link}", link, ST * T * 2, ["mixsum"],
+    for j in (2, 1, 3, 0):
+        ev.append(Event(f"Q{j}", "p", ST * T * 2, [f"mix{j}"], lambda j=j: preo.at[j], lambda j=j: prei.at[j]))
+    for link, j in (("xx", 2), ("x+", 1), ("x-", 3)):
+        ev.append(Event(f"R{link}", link, ST * T * 2, [f"mixsum{j}"],
                         lambda j=j: rxo.at[j - 1], lambda j=j: rxi.at[j - 1]))
     all_x2 = spread("X2", X2, "after")
     for g in range(4):
@@ -232,10 +269,11 @@
             else:
                 n -= 8
                 G2[(*own, slice(None), slice(128 * n, 128 * n + 128))] = pair[k]
-    D1[own] = (dw[0:384] * ds[...]).T.astype(BF)
-    D2[(*own, slice(None), slice(0, 256))] = (dw[384:640] * ds[...]).T.astype(BF)
-    tail = (dw[640:704] * ds[...]).T
-    D2[(*own, slice(None), slice(256, 384))] = jnp.concatenate([tail, jnp.zeros((64, 64), F32)], axis=1).astype(BF)
+    rescale = ds[...].T
+    D1[own] = (dw[:, 0:256] * rescale).astype(BF)
+    D2[(*own, slice(None), slice(0, 384))] = (dw[:, 256:640] * rescale).astype(BF)
+    tail = jnp.concatenate([dw[:, 640:704] * rescale, jnp.zeros((64, 64), F32)], axis=1)
+    D2[(*own, slice(None), slice(384, 512))] = tail.astype(BF)
     row = vs[...] * ivs[...] * ovs[...]
     for k in range(3):
         line = taps[k:k + 1] * row
@@ -298,36 +336,40 @@
         stat = (lax.dot_general(ones, high, nt, preferred_element_type=F32)
                 + lax.dot_general(ones, low, nt, preferred_element_type=F32))[:8]
         scaled = (mixed * small[3:4]).astype(BF)
-        for j in range(4):
-            for mine in (False, True):
-                core = c if mine else 1 - c
-                w = M[lax.rem(x + j, 4), pl.ds(4 * core, 4), :, 128:].reshape(256, 128)
-                part = lax.dot_general(w, scaled, nt, preferred_element_type=F32)
-                if mine:
-                    own32[j] = part
-                else:
-                    preo[j, :256] = part.astype(BF)
-                    preo[j, 256:] = split_stats(stat)
+        mixed_to[...] = scaled
         keep[0:8] = stat
 
-    def mixsum():
+    def mix_for(j):
+        nt = (((1,), (1,)), ((), ()))
+        for mine in (False, True):
+            core = c if mine else 1 - c
+            w = M[lax.rem(x + j, 4), pl.ds(4 * core, 4), :, 128:].reshape(256, 128)
+            part = lax.dot_general(w, mixed_to[...], nt, preferred_element_type=F32)
+            if mine:
+                own32[j] = part
+            else:
+                preo[j, :256] = part.astype(BF)
+                preo[j, 256:] = split_stats(keep[0:8])
+
+    def mix_first():
+        mix()
+        mix_for(2)
+
+    def mixsum(j):
+        stat = keep[0:8] + prei[j, 256:264].astype(F32) + prei[j, 264:272].astype(F32)
+        rxo[j - 1, :256] = (own32[j] + prei[j, :256].astype(F32)).astype(BF)
+        rxo[j - 1, 256:] = split_stats(stat)
+
+    def after():
         stat = keep[0:8] + prei[0, 256:264].astype(F32) + prei[0, 264:272].astype(F32)
-        for j in (2, 1, 3):
-            rxo[j - 1, :256] = (own32[j] + prei[j, :256].astype(F32)).astype(BF)
-            rxo[j - 1, 256:] = split_stats(stat)
-        own32[0] = own32[0] + prei[0, :256].astype(F32)
-        keep[0:8] = stat
-
-    def after():
-        stat = keep[0:8]
-        total = own32[0]
+        total = own32[0] + prei[0, :256].astype(F32)
         for j in range(3):
             total = total + rxi[j, :256].astype(F32)
             stat = stat + rxi[j, 256:264].astype(F32) + rxi[j, 264:272].astype(F32)
         factor = lax.rsqrt(stat * (1.0 / 512) + EPS)[0:1]
         value = (res[...].astype(F32) + total * factor).astype(BF)
         X2[slot(0, c)] = value.astype(F32).T.astype(BF)
-        out[...] = value
+        out[...] = value.astype(F32)
 
     def norm_two():
         normed(X2, cgain)
@@ -341,11 +383,11 @@
             even = z[:, 128 * k:128 * k + 128]
             if k + 1 < tiles:
                 odd = z[:, 128 * k + 128:128 * k + 256]
-                gsc, usc = gs[0:1, 128 * n:128 * n + 128], us[0:1, 128 * n:128 * n + 128]
+                gsc, usc = (v[128 * n:128 * n + 128].reshape(1, 128) for v in (gs, us))
             else:
                 odd = jnp.zeros((T, 128), F32)
-                gsc = jnp.concatenate([gs[0:1, 640:704]] * 2, axis=1)
-                usc = jnp.concatenate([us[0:1, 640:704]] * 2, axis=1)
+                gsc = jnp.concatenate([gs[640:704].reshape(1, 64)] * 2, axis=1)
+                usc = jnp.concatenate([us[640:704].reshape(1, 64)] * 2, axis=1)
             gate = jnp.where(lane < 64, even, odd) * gsc
             up = pltpu.roll(jnp.where(lane < 64, odd, even), 64, axis=1) * usc
             hid[:, 128 * n:128 * n + 128] = (gate / (1.0 + jnp.exp(-gate)) * up).astype(BF)
@@ -361,8 +403,8 @@
     def down(g, core):
         at = lax.rem(y + g, 4) + 4 * core
         nt = (((1,), (1,)), ((), ()))
-        p = lax.dot_general(D1[:, at].reshape(256, DL), hid[:, :DL], nt, preferred_element_type=F32)
-        q = lax.dot_general(D2[:, at].reshape(256, DL), hid[:, DL:], nt, preferred_element_type=F32)
+        p = lax.dot_general(D1[:, at].reshape(256, D1L), hid[:, :D1L], nt, preferred_element_type=F32)
+        q = lax.dot_general(D2[:, at].reshape(256, D2L), hid[:, D1L:], nt, preferred_element_type=F32)
         return (p + q).reshape(4, 64, T)
 
     def down_partner(g):
@@ -381,23 +423,28 @@
         total = own32[g, pl.ds(pl.multiple_of(x * 64, 64), 64)] + qi[g, x].astype(F32)
         for j in range(3):
             total = total + ri[g, j].astype(F32)
-        out[rows] = (out[rows].astype(F32) + total).astype(BF)
+        out[rows] = out[rows] + total
 
     tasks = [
         ("norm1", all_x1, 0.8, norm_one),
-        ("mix", ["norm1"] + all_m, 1.5, mix),
-        ("mixsum", ["Q"], 0.5, mixsum),
-        ("after", ["Rx+", "Rx-", "Rxx"], 0.5, after),
+        ("mix2", ["norm1"] + all_m, 1.0, mix_first),
+        ("mix1", ["mix2"], 0.2, lambda: mix_for(1)),
+        ("mix3", ["mix1"], 0.2, lambda: mix_for(3)),
+        ("mix0", ["mix3"], 0.2, lambda: mix_for(0)),
+        ("mixsum2", ["Q2", "mix0"], 0.05, lambda: mixsum(2)),
+        ("mixsum1", ["Q1", "mix0"], 0.05, lambda: mixsum(1)),
+        ("mixsum3", ["Q3", "mix0"], 0.05, lambda: mixsum(3)),
+        ("after", ["Q0", "mixsum2", "mixsum1", "mixsum3", "Rx+", "Rx-", "Rxx"], 0.2, after),
         ("norm2", all_x2, 0.8, norm_two),
         ("hidden1", ["norm2"] + all_g, 1.4, hidden_one),
-        ("hidden2", ["norm2"] + all_h, 0.6, hidden_two),
+        ("hidden2", ["norm2"] + all_h, 0.8, hidden_two),
     ]
-    for g in (2, 1, 3, 0):
+    for g in GROUPS:
         need = of_y[g] + (of_y[g - 4] if g else of_y[4])
         tasks.append((f"down{g}", ["hidden1", "hidden2"] + need, 0.4, lambda g=g: down_partner(g)))
         tasks.append((f"own{g}", [f"down{g}"], 0.4, lambda g=g: down_own(g)))
         tasks.append((f"sum{g}", [f"own{g}", f"S{g}"], 0.2, lambda g=g: sum_for(g)))
-    for g in (2, 1, 3, 0):
+    for g in GROUPS:
         tasks.append((f"final{g}", [f"U{g}x+", f"U{g}x-", f"U{g}xx"], 0.1, lambda g=g: final(g)))
     order = plan(ev, tasks)
     for kind, item in order:
@@ -411,7 +458,7 @@
         left(e)
 
 
-N_EVENTS = 12 + 40 + 12 + 12 + 40 + 7 + 1 + 3 + 7 + 4 + 12
+N_EVENTS = 12 + 40 + 12 + 12 + 40 + 7 + 4 + 3 + 7 + 4 + 12
 
 
 def local(residual, mixer_gain, value_weight, value_scale, input_gate_weight, input_gate_scale,
@@ -425,20 +472,20 @@
     V = pltpu.VMEM
     return pl.pallas_call(
         functools.partial(kernel, n_events=N_EVENTS),
-        out_shape=jax.ShapeDtypeStruct((256, T), BF),
+        out_shape=jax.ShapeDtypeStruct((256, T), F32),
         in_specs=[hbm] * 19,
         out_specs=vmem,
         scratch_shapes=[
             V((4, 8, 64, NM), BF), V((4, 8, 64, G1L), BF), V((4, 8, 64, G2L), BF),
-            V((4, 8, 64, DL), BF), V((4, 8, 64, DL), BF),
-            V((8, T, 256), BF), V((8, T, 256), BF), V((T, 2048), BF), V((T, 2 * DL), BF),
-            V((8, T), F32), V((4, 256, T), F32),
+            V((4, 8, 64, D1L), BF), V((4, 8, 64, D2L), BF),
+            V((8, T, 256), BF), V((8, T, 256), BF), V((T, 2048), BF), V((T, D1L + D2L), BF),
+            V((8, T), F32), V((T, 128), BF), V((4, 256, T), F32),
             V((4, ST, T), BF), V((4, ST, T), BF), V((3, ST, T), BF), V((3, ST, T), BF),
             V((4, 4, 64, T), BF), V((4, 4, 64, T), BF), V((4, 3, 64, T), BF), V((4, 3, 64, T), BF),
             V((256, T), BF), V((1, 2048), F32), V((1, 2048), F32), V((64, 64), F32), V((64, 64), F32),
-            V((64, 64), F32), V((64, 64), F32), V((64, FFL), F32), V((64, FFL), F32), V((FFL, 64), F32),
+            V((64, 64), F32), V((64, 64), F32), V((64, FFL), F32), V((64, FFL), F32), V((64, FFL), F32),
             V((1, 64), F32), V((1, 64), F32), V((1, 64), F32), V((3, 64), F32), V((1, 64), F32), V((1, 64), F32),
-            V((1, FFL), F32), V((1, FFL), F32), V((1, 64), F32), V((8, 128), F32),
+            V((FFL,), F32), V((FFL,), F32), V((1, 64), F32), V((8, 128), F32),
             pltpu.SemaphoreType.DMA((N_EVENTS,)), pltpu.SemaphoreType.DMA((N_EVENTS,)),
             pltpu.SemaphoreType.DMA((19,)),
         ],
@@ -446,9 +493,9 @@
                                              vmem_limit_bytes=60 * 1024 * 1024),
         name="layer",
     )(residual, line(mixer_gain), line(channel_gain), value_weight, input_gate_weight, output_gate_weight,
-      mixer_out_weight, gate_weight, up_weight, down_weight, line(value_scale), line(input_gate_scale),
-      line(output_gate_scale), conv_taps, line(conv_gain), line(mixer_out_scale), line(gate_scale),
-      line(up_scale), line(down_scale))
+      mixer_out_weight, gate_weight, up_weight, down_weight.T, line(value_scale), line(input_gate_scale),
+      line(output_gate_scale), conv_taps, line(conv_gain), line(mixer_out_scale), gate_scale,
+      up_scale, line(down_scale)).astype(BF)
 
 
 def solution(mesh):

time: 95.8 us -> 84.1 us (0.88)
  Pallas kernels: 90.4 us -> 82.3 us
  local copies, waits for them, and re-layouts: 5.26 us -> 0 us
  other arithmetic: 0 us -> 1.62 us
    pallas_call x1, Pallas kernels: 90.4 us -> 82.3 us  [local(): pl.pallas_call(functools.partial(kernel, n_events=N_EVENTS), out_shape=ja...]
    unnamed x6 -> x0, local copies, waits for them, and re-layouts: 4.08 us -> none
    convert_element_type x0 -> x1, other arithmetic: none -> 1.62 us  [local(): return pl.pallas_call(functools.partial(kernel, n_events=N_EVENTS), out_s...]
    reshape x2 -> x0, local copies, waits for them, and re-layouts: 1.18 us -> none  [line(): return a.reshape(1, -1)]
where the time goes in v3:
time: 84.1 us; the launch traced here: 83.9 us
  Pallas kernels  82.3 us (98%)
  other arithmetic  1.62 us (2%)
    pallas_call x1, Pallas kernels, local(): pl.pallas_call(functools.partial(kernel, n_events=N_EVENTS), out_shape=ja...  82.3 us

profile of v3, /device:TPU:1, one launch (start us, length us, event | category | flops | bytes accessed | tf_op | source)
XLA Modules:
  0.0 83.9 jit_solution(15809765883363442689)
XLA Ops:
  0.0 82.3 %layer.1 = f32[256,256]{1,0:T(8,128)} custom-call(bf16[256,256]{1,0:T(8,128)(2,1)} %res_in.1, f32[1,2048]{1,0:T(1,128)} %bitcast.10, f32[1,2048]{1,0:T(1,128)} %bitcast.11, f32[64,64]{1,0:T(8,128)} %v_in.1, f32[64,64]{1,0:T(8,128)} %i_in.1, f32[64,64]{1,0:T(8,128)} %o_in.1, f32[64,64]{1,0:T(8,128)} %w_in.1, f32[64,704]{1,0:T(8,128)} %g_in.1, ...), custom_call_target="tpu_custom_call" | custom-call | tf_op jit(solution)/shard_map/layer/pallas_call | solution.py:473
  82.3 1.6 %convert_element_type.3 = bf16[256,256]{1,0:T(8,128)(2,1)} convert(f32[256,256]{1,0:T(8,128)} %layer.1) | non-fusion elementwise | flops 65536 | bytes 393216 | tf_op jit(solution)/shard_map/convert_element_type | solution.py:498

commit v4 on v3

--- a/solution.py
+++ b/solution.py
@@ -26,6 +26,27 @@
 
 RATE = {"p": 100.0, "xx": 28.0, "x+": 60.0, "x-": 60.0}
 LAT = {"p": 1.5, "xx": 2.6}
+
+
+def landing(name):
+    kind, last = name[0], name[-1]
+    if kind == "G" and "z" in name and last == "2":
+        return "Gz2"
+    if kind == "E" and "z" in name and last == "2":
+        return f"Ez2{int(name[1:name.index('z')]) % 4}"
+    if kind in "MHD" and "y" in name and last == "4":
+        return kind + "y4"
+    if kind == "X" and name[2] == "p":
+        return name[:3]
+    if kind in "RU":
+        return name[:1 if kind == "R" else 2]
+    return name
+
+
+def leaving(name):
+    if name[0] in "XQRSU":
+        return name[:2] if name[0] == "X" else name[0]
+    return name[0] + ("z" if "z" in name else "y")
 
 
 def plan(events, tasks):
@@ -57,8 +78,8 @@
             t = ready[0]
             left.remove(t)
             for d in t[1]:
-                if d in by_name and d not in waited:
-                    waited.add(d)
+                if d in by_name and landing(d) not in waited:
+                    waited.add(landing(d))
                     order.append(("wait", by_name[d]))
             order.append(("run", t))
             now += t[2]
@@ -69,8 +90,8 @@
             f = min(flights, key=lambda v: v[0])
             now = f[0]
         flights.remove(f)
-        if f[1].name in passed_on:
-            waited.add(f[1].name)
+        if f[1].name in passed_on and landing(f[1].name) not in waited:
+            waited.add(landing(f[1].name))
             order.append(("wait", f[1]))
         done.add(f[1].name)
         launch()
@@ -84,6 +105,7 @@
         ev.append(Event(name, link, size, deps, lambda: ref(*W.shift[link]), lambda: ref(0, 0)))
 
     def along_z(tag, buf, width, b, have):
+        have = have or CAST.get(tag[0], [])
         size = 64 * width * 2
         for sign, link in ((-1, "z+"), (1, "z-")):
             add(f"{tag}{link}1", link, size, have, lambda dz, dy, s=sign: buf.at[W.zl(s + dz), W.yy(b + dy)])
@@ -112,7 +134,7 @@
             for sign, link, lo in ((-1, "y+", 0), (1, "y-", 32)):
                 n, at = (64, 0) if s < 4 else (32, lo)
                 add(f"{tag}{link}{s}", link, n * width * 2,
-                    ([] if s == 1 else [f"{tag}{link}{s - 1}"]) + gate(tag, s, link),
+                    (CAST[tag] if s == 1 else [f"{tag}{link}{s - 1}"]) + gate(tag, s, link),
                     lambda dz, dy, s=s, sign=sign, at=at, n=n: buf.at[W.zl(dz), W.yy(sign * s + dy), pl.ds(at, n)])
 
     def behind(tag, b):
@@ -151,10 +173,11 @@
                 need["G"] += behind("G", b) + along_z(f"G{b}", G1, G1L, b, behind("G", b))
         else:
             for b in LAST:
-                of_y[b] = of_y[b] + behind("E", b) + along_z(f"E{b}", D2, D2L, b, behind("E", b) + z_names(HOLD)[:2])
+                of_y[b] = of_y[b] + behind("E", b) + along_z(f"E{b}", D2, D2L, b, CAST["E"] + behind("E", b) + z_names(HOLD)[:2])
     return ev, need["M"], need["G"], need["H"], of_y
 
 
+CAST = {"G": ["castG"], "H": ["castG"], "D": ["castD"], "E": ["castD"]}
 FIRST = ("Hz", "M", "H", "E", "Gz", "Dz", "Ez", "G", "D")
 LAST = (2, -2, 3, -1, -3, 4, 1, 0)
 HOLD = "G4"
@@ -234,7 +257,6 @@
             ev.append(Event(f"U{g}{link}", link, 64 * T * 2, [f"sum{g}"],
                             lambda j=j, g=g: ro.at[g, j - 1], lambda j=j, g=g: ri.at[g, j - 1]))
     assert len(ev) == n_events, len(ev)
-    index = {e.name: i for i, e in enumerate(ev)}
 
     barrier = pltpu.get_barrier_semaphore()
     for dev in target.values():
@@ -246,59 +268,87 @@
     copies = [pltpu.make_async_copy(src, dst, loc_sem.at[i]) for i, (src, dst) in enumerate(ins)]
     for copy in copies:
         copy.start()
-    for copy in copies:
-        copy.wait()
-    half = lax.broadcasted_iota(jnp.int32, (64, 128), 1) < 64
+    def ready(*which):
+        for i in which:
+            copies[i].wait()
+
+    own = (zl, y)
+    ready(0, 1, 2, 3, 4, 5)
     X1[slot(0, c)] = res[...].astype(F32).T.astype(BF)
-    own = (zl, y)
     M[(*own, slice(None), slice(0, 128))] = jnp.concatenate([vw[...], iw[...]], axis=1).astype(BF)
     turned = (mw[...] * ms[...]).T
     M[(*own, slice(None), slice(128, 256))] = jnp.concatenate([ow[...], turned], axis=1).astype(BF)
-    for t in range(6):
-        if t < 5:
-            gate, up = gw[:, 128 * t:128 * t + 128], uw[:, 128 * t:128 * t + 128]
+
+    def cast_gate_up():
+        ready(6, 7)
+        half = lax.broadcasted_iota(jnp.int32, (64, 128), 1) < 64
+        for t in range(6):
+            if t < 5:
+                gate, up = gw[:, 128 * t:128 * t + 128], uw[:, 128 * t:128 * t + 128]
+            else:
+                gate = jnp.concatenate([gw[:, 640:704]] * 2, axis=1)
+                up = jnp.concatenate([uw[:, 640:704]] * 2, axis=1)
+            turn = pltpu.roll(up, 64, axis=1)
+            pair = [jnp.where(half, gate, turn).astype(BF), jnp.where(half, turn, gate).astype(BF)]
+            for k in range(2 if t < 5 else 1):
+                n = 2 * t + k
+                if n < G1L // 128:
+                    G1[(*own, slice(None), slice(128 * n, 128 * n + 128))] = pair[k]
+                else:
+                    n -= G1L // 128
+                    G2[(*own, slice(None), slice(128 * n, 128 * n + 128))] = pair[k]
+
+    def cast_down():
+        ready(8, 9)
+        rescale = ds[...].T
+        D1[own] = (dw[:, 0:256] * rescale).astype(BF)
+        D2[(*own, slice(None), slice(0, 384))] = (dw[:, 256:640] * rescale).astype(BF)
+        tail = jnp.concatenate([dw[:, 640:704] * rescale, jnp.zeros((64, 64), F32)], axis=1)
+        D2[(*own, slice(None), slice(384, 512))] = tail.astype(BF)
+        ready(*range(10, 19))
+        row = vs[...] * ivs[...] * ovs[...]
+        for k in range(3):
+            line = taps[k:k + 1] * row
+            small[k:k + 1] = jnp.concatenate([line, line], axis=1)
+        small[3:4] = jnp.concatenate([cg[...], cg[...]], axis=1)
+
+    pl.semaphore_wait(barrier, 8)
+
+    bufs = {"M": M, "G": G1, "H": G2, "D": D1, "E": D2}
+    out_total = {"X1": X1.at[:7], "X2": X2.at[:7], "Q": preo, "R": rxo, "S": qo, "U": ro}
+    in_total = {"Gz2": G1.at[0], "X1p": X1.at[:4], "X2p": X2.at[:4], "R": rxi}
+    for k, buf in bufs.items():
+        if k in "MHD":
+            out_total[k + "z"], out_total[k + "y"] = buf.at[0, :3], buf.at[:, :7]
+            in_total[k + "y4"] = buf.at[:, 0]
         else:
-            gate = jnp.concatenate([gw[:, 640:704]] * 2, axis=1)
-            up = jnp.concatenate([uw[:, 640:704]] * 2, axis=1)
-        turn = pltpu.roll(up, 64, axis=1)
-        pair = [jnp.where(half, gate, turn).astype(BF), jnp.where(half, turn, gate).astype(BF)]
-        for k in range(2 if t < 5 else 1):
-            n = 2 * t + k
-            if n < 8:
-                G1[(*own, slice(None), slice(128 * n, 128 * n + 128))] = pair[k]
-            else:
-                n -= 8
-                G2[(*own, slice(None), slice(128 * n, 128 * n + 128))] = pair[k]
-    rescale = ds[...].T
-    D1[own] = (dw[:, 0:256] * rescale).astype(BF)
-    D2[(*own, slice(None), slice(0, 384))] = (dw[:, 256:640] * rescale).astype(BF)
-    tail = jnp.concatenate([dw[:, 640:704] * rescale, jnp.zeros((64, 64), F32)], axis=1)
-    D2[(*own, slice(None), slice(384, 512))] = tail.astype(BF)
-    row = vs[...] * ivs[...] * ovs[...]
-    for k in range(3):
-        line = taps[k:k + 1] * row
-        small[k:k + 1] = jnp.concatenate([line, line], axis=1)
-    small[3:4] = jnp.concatenate([cg[...], cg[...]], axis=1)
-    pl.semaphore_wait(barrier, 8)
+            out_total[k + "z"], out_total[k + "y"] = buf.at[:3], buf.at[0, :7]
+    for g in range(4):
+        in_total[f"Ez2{g}"] = D2.at[0, :2]
+        in_total[f"U{g}"] = ri.at[g]
+    out_index = {k: i for i, k in enumerate(out_total)}
+    in_index = {k: i for i, k in enumerate(dict.fromkeys(landing(e.name) for e in ev))}
+    assert len(out_index) == N_OUT and len(in_index) == N_IN, (len(out_index), len(in_index))
 
     def start(e):
-        i = index[e.name]
         ref = e.put()
-        pltpu.make_async_remote_copy(src_ref=ref, dst_ref=ref if e.link[0] in "yz" or e.name[:1] == "X" else e.got(),
-                                     send_sem=send_sem.at[i], recv_sem=recv_sem.at[i],
-                                     device_id=target[e.link], device_id_type=MESH).start()
+        pltpu.make_async_remote_copy(
+            src_ref=ref, dst_ref=ref if e.link[0] in "yz" or e.name[:1] == "X" else e.got(),
+            send_sem=send_sem.at[out_index[leaving(e.name)]], recv_sem=recv_sem.at[in_index[landing(e.name)]],
+            device_id=target[e.link], device_id_type=MESH).start()
 
     def arrive(e):
-        i = index[e.name]
-        ref = e.got()
-        pltpu.make_async_remote_copy(src_ref=ref, dst_ref=ref, send_sem=send_sem.at[i], recv_sem=recv_sem.at[i],
+        key = landing(e.name)
+        ref = in_total[key] if key in in_total else e.got()
+        pltpu.make_async_remote_copy(src_ref=ref, dst_ref=ref, send_sem=send_sem.at[0],
+                                     recv_sem=recv_sem.at[in_index[key]],
                                      device_id=target[e.link], device_id_type=MESH).wait_recv()
 
-    def left(e):
-        i = index[e.name]
-        ref = e.put()
-        pltpu.make_async_remote_copy(src_ref=ref, dst_ref=ref, send_sem=send_sem.at[i], recv_sem=recv_sem.at[i],
-                                     device_id=target[e.link], device_id_type=MESH).wait_send()
+    def left():
+        for key, i in out_index.items():
+            ref = out_total[key]
+            pltpu.make_async_remote_copy(src_ref=ref, dst_ref=ref, send_sem=send_sem.at[i], recv_sem=recv_sem.at[0],
+                                         device_id=partner, device_id_type=MESH).wait_send()
 
     def normed(buf, gain):
         def square(k, s):
@@ -426,6 +476,8 @@
         out[rows] = out[rows] + total
 
     tasks = [
+        ("castG", [], 0.4, cast_gate_up),
+        ("castD", ["castG"], 0.4, cast_down),
         ("norm1", all_x1, 0.8, norm_one),
         ("mix2", ["norm1"] + all_m, 1.0, mix_first),
         ("mix1", ["mix2"], 0.2, lambda: mix_for(1)),
@@ -454,11 +506,11 @@
             arrive(item)
         else:
             item[3]()
-    for e in ev:
-        left(e)
+    left()
 
 
 N_EVENTS = 12 + 40 + 12 + 12 + 40 + 7 + 4 + 3 + 7 + 4 + 12
+N_OUT, N_IN = 16, 107
 
 
 def local(residual, mixer_gain, value_weight, value_scale, input_gate_weight, input_gate_scale,
@@ -472,7 +524,7 @@
     V = pltpu.VMEM
     return pl.pallas_call(
         functools.partial(kernel, n_events=N_EVENTS),
-        out_shape=jax.ShapeDtypeStruct((256, T), F32),
+        out_shape=V((256, T), F32),
         in_specs=[hbm] * 19,
         out_specs=vmem,
         scratch_shapes=[
@@ -486,7 +538,7 @@
             V((64, 64), F32), V((64, 64), F32), V((64, FFL), F32), V((64, FFL), F32), V((64, FFL), F32),
             V((1, 64), F32), V((1, 64), F32), V((1, 64), F32), V((3, 64), F32), V((1, 64), F32), V((1, 64), F32),
             V((FFL,), F32), V((FFL,), F32), V((1, 64), F32), V((8, 128), F32),
-            pltpu.SemaphoreType.DMA((N_EVENTS,)), pltpu.SemaphoreType.DMA((N_EVENTS,)),
+            pltpu.SemaphoreType.DMA((N_OUT,)), pltpu.SemaphoreType.DMA((N_IN,)),
             pltpu.SemaphoreType.DMA((19,)),
         ],
         compiler_params=pltpu.CompilerParams(collective_id=0, has_side_effects=True,

time: 84.1 us -> 79.9 us (0.950)
  Pallas kernels: 82.3 us -> 79.1 us
  other arithmetic: 1.62 us -> 0.67 us
    pallas_call x1, Pallas kernels: 82.3 us -> 79.1 us  [local(): pl.pallas_call(functools.partial(kernel, n_events=N_EVENTS), out_shape=V(...]
    convert_element_type x1, other arithmetic: 1.62 us -> 0.67 us  [local(): return pl.pallas_call(functools.partial(kernel, n_events=N_EVENTS), out_s...]
where the time goes in v4:
time: 79.9 us; the launch traced here: 79.8 us
  Pallas kernels  79.1 us (99%)
    pallas_call x1, Pallas kernels, local(): pl.pallas_call(functools.partial(kernel, n_events=N_EVENTS), out_shape=V(...  79.1 us

profile of v4, /device:TPU:1, one launch (start us, length us, event | category | flops | bytes accessed | tf_op | source)
XLA Modules:
  0.0 79.8 jit_solution(12082153730022168785)
XLA Ops:
  0.0 79.1 %layer.1 = f32[256,256]{1,0:T(8,128)S(1)} custom-call(bf16[256,256]{1,0:T(8,128)(2,1)} %res_in.1, f32[1,2048]{1,0:T(1,128)} %bitcast.10, f32[1,2048]{1,0:T(1,128)} %bitcast.11, f32[64,64]{1,0:T(8,128)} %v_in.1, f32[64,64]{1,0:T(8,128)} %i_in.1, f32[64,64]{1,0:T(8,128)} %o_in.1, f32[64,64]{1,0:T(8,128)} %w_in.1, f32[64,704]{1,0:T(8,128)} %g_in.1, ...), custom_call_target="tpu_custom_call" | custom-call | tf_op jit(solution)/shard_map/layer/pallas_call | solution.py:525
  79.1 0.7 convert_element_type.3

commit v5 on v4

--- a/solution.py
+++ b/solution.py
@@ -13,8 +13,9 @@
 EPS = 1e-06
 LEN = 128
 T = 256
-NM, G1L, G2L, D1L, D2L = 256, 1024, 384, 256, 512
+NM, G1L, G2L, D1L, D2L = 256, 1024, 384, 256, 384
 FFL = 704
+DROWS = 80
 ST = 272
 
 
@@ -24,8 +25,8 @@
         self.put, self.got = put, got
 
 
-RATE = {"p": 100.0, "xx": 28.0, "x+": 60.0, "x-": 60.0}
-LAT = {"p": 1.5, "xx": 2.6}
+RATE = {"p": 90.0, "xx": 25.0, "x+": 40.0}
+LAT = {"p": 1.7, "xx": 2.8}
 
 
 def landing(name):
@@ -34,8 +35,8 @@
         return "Gz2"
     if kind == "E" and "z" in name and last == "2":
         return f"Ez2{int(name[1:name.index('z')]) % 4}"
-    if kind in "MHD" and "y" in name and last == "4":
-        return kind + "y4"
+    if kind in "MHDmhd" and "y" in name and last == "4":
+        return kind.upper() + "y4"
     if kind == "X" and name[2] == "p":
         return name[:3]
     if kind in "RU":
@@ -46,7 +47,7 @@
 def leaving(name):
     if name[0] in "XQRSU":
         return name[:2] if name[0] == "X" else name[0]
-    return name[0] + ("z" if "z" in name else "y")
+    return name[0].upper() + ("z" if "z" in name else "y")
 
 
 def plan(events, tasks):
@@ -61,10 +62,10 @@
         for e in events:
             if e.name not in sent and all(d in done for d in e.deps):
                 sent.add(e.name)
-                start = max(now, free.get(e.link, 0.0))
+                start = max(now, free.get(e.link[:2], 0.0))
                 end = start + e.size / (RATE.get(e.link, 46.0) * 1e3)
-                free[e.link] = end
-                flights.append((end + LAT.get(e.link, 1.8), e))
+                free[e.link[:2]] = end
+                flights.append((end + LAT.get(e.link, 2.0), e))
                 order.append(("send", e))
 
     launch()
@@ -105,28 +106,42 @@
         ev.append(Event(name, link, size, deps, lambda: ref(*W.shift[link]), lambda: ref(0, 0)))
 
     def along_z(tag, buf, width, b, have):
+        rows = buf.shape[2]
+        mid = 32 if rows == 64 else 48
         have = have or CAST.get(tag[0], [])
-        size = 64 * width * 2
+        size = rows * width * 2
         for sign, link in ((-1, "z+"), (1, "z-")):
             add(f"{tag}{link}1", link, size, have, lambda dz, dy, s=sign: buf.at[W.zl(s + dz), W.yy(b + dy)])
-        for sign, link, lo in ((-1, "z+", 0), (1, "z-", 32)):
-            add(f"{tag}{link}2", link, size // 2, [f"{tag}{link}1"],
-                lambda dz, dy, s=sign, lo=lo: buf.at[W.zl(2 * s + dz), W.yy(b + dy), pl.ds(lo, 32)])
+        for sign, link, lo, n in ((-1, "z+", 0, mid), (1, "z-", mid, rows - mid)):
+            if tag == "M":
+                ev.append(Event(f"{tag}{link}2", link + link[1], 2 * n * width * 2, [],
+                                lambda lo=lo, n=n: buf.at[W.zl(0), W.yy(0), pl.ds(lo, n)],
+                                lambda s=sign, lo=lo, n=n: buf.at[W.zl(2 * s), W.yy(0), pl.ds(lo, n)]))
+                continue
+            add(f"{tag}{link}2", link, n * width * 2, [f"{tag}{link}1"],
+                lambda dz, dy, s=sign, lo=lo, n=n: buf.at[W.zl(2 * s + dz), W.yy(b + dy), pl.ds(lo, n)])
         return [f"{tag}z+1", f"{tag}z-1", f"{tag}z+2", f"{tag}z-2"]
 
     def gate(tag, s, link):
         other = GATE.get(f"{tag}{s}")
-        return [f"{other[0]}{link}{other[1]}"] if other else []
+        if not other:
+            return []
+        kind = other[0]
+        if other[1] == "4" and kind in "MHD" and link == "y-":
+            kind = kind.lower()
+        return [f"{kind}{link}{other[1]}"]
 
     def columns_along_y(tag, buf, width, first):
         names = []
         for s in (1, 2, 3, 4):
-            for sign, link, lo in ((-1, "y+", 0), (1, "y-", 2)):
-                n, at = (4, 0) if s < 4 else (2, lo)
-                add(f"{tag}{link}{s}", link, n * 64 * width * 2,
-                    (first if s == 1 else [f"{tag}{link}{s - 1}"]) + gate(tag, s, link),
-                    lambda dz, dy, s=s, sign=sign, at=at, n=n: buf.at[pl.ds(at, n), W.yy(sign * s + dy)])
-                names.append(f"{tag}{link}{s}")
+            for t, at in ((tag, 0), (tag.lower(), 2)):
+                for sign, link in ((-1, "y+"), (1, "y-")):
+                    if s == 4 and (t == tag) != (link == "y+"):
+                        continue
+                    add(f"{t}{link}{s}", link, 2 * buf.shape[2] * width * 2,
+                        (first if s == 1 else [f"{t}{link}{s - 1}"]) + gate(tag, s, link),
+                        lambda dz, dy, s=s, sign=sign, at=at: buf.at[pl.ds(at, 2), W.yy(sign * s + dy)])
+                    names.append(f"{t}{link}{s}")
         return names
 
     def own_along_y(tag, buf, width):
@@ -148,10 +163,10 @@
         return [f"{tag}z+1", f"{tag}z-1", f"{tag}z+2", f"{tag}z-2"]
 
     need = {}
-    of_y = {0: z_names("D"), 4: ["Dy+4", "Dy-4"]}
+    of_y = {0: z_names("D"), 4: ["Dy+4", "dy-4"]}
     for s in (1, 2, 3):
-        of_y[-s] = [f"Dy+{s}"]
-        of_y[s] = [f"Dy-{s}"]
+        of_y[-s] = [f"Dy+{s}", f"dy+{s}"]
+        of_y[s] = [f"Dy-{s}", f"dy-{s}"]
     for part in FIRST:
         if part == "M":
             need["M"] = along_z("M", M, NM, 0, []) + columns_along_y("M", M, NM, z_names("M"))
@@ -178,13 +193,13 @@
 
 
 CAST = {"G": ["castG"], "H": ["castG"], "D": ["castD"], "E": ["castD"]}
-FIRST = ("Hz", "M", "H", "E", "Gz", "Dz", "Ez", "G", "D")
-LAST = (2, -2, 3, -1, -3, 4, 1, 0)
+FIRST = ("Ez", "D", "Hz", "M", "Gz", "E", "H", "G", "Dz")
+LAST = (0, -2, 2, 4, -3, 3, -1, 1)
 HOLD = "G4"
 GROUPS = (2, 1, 0, 3)
 GATE = {
-    "H1": "M3", "E2": "G4", "D1": "H1", "M2": "E1", "G3": "G2", "H3": "E2", "D2": "G3", "E3": "E1", "D3":
-    "D1", "G4": "G3", "H2": "M4",
+    "H1": "G4", "D2": "H3", "E1": "G3", "D3": "D2", "D1": "E2", "H3": "H2", "E2": "M2", "G4": "G2", "E3":
+    "H1", "H2": "M4", "M2": "M1",
 }
 
 
@@ -213,7 +228,7 @@
         return {"tp": lax.rem(x + d + 4, 4) * 2 + c}
 
     partner = {"tp": x * 2 + 1 - c}
-    target = {"y+": y_at(1), "y-": y_at(-1), "z+": z_at(1), "z-": z_at(-1),
+    target = {"y+": y_at(1), "y-": y_at(-1), "z+": z_at(1), "z-": z_at(-1), "z++": z_at(2), "z--": z_at(-2),
               "x+": x_at(1), "x-": x_at(-1), "xx": x_at(2), "p": partner}
 
     W = Where()
@@ -301,10 +316,11 @@
     def cast_down():
         ready(8, 9)
         rescale = ds[...].T
-        D1[own] = (dw[:, 0:256] * rescale).astype(BF)
-        D2[(*own, slice(None), slice(0, 384))] = (dw[:, 256:640] * rescale).astype(BF)
-        tail = jnp.concatenate([dw[:, 640:704] * rescale, jnp.zeros((64, 64), F32)], axis=1)
-        D2[(*own, slice(None), slice(384, 512))] = tail.astype(BF)
+        D1[(*own, slice(0, 64))] = (dw[:, 0:256] * rescale).astype(BF)
+        D2[own] = (dw[:, 256:640] * rescale).astype(BF)
+        tail = dw[:, 640:704] * rescale
+        fold = [jnp.concatenate([tail[32 * k:32 * k + 16], tail[32 * k + 16:32 * k + 32]], axis=1) for k in range(2)]
+        D1[(*own, slice(64, 80))] = jnp.concatenate(fold, axis=1).astype(BF)
         ready(*range(10, 19))
         row = vs[...] * ivs[...] * ovs[...]
         for k in range(3):
@@ -312,7 +328,7 @@
             small[k:k + 1] = jnp.concatenate([line, line], axis=1)
         small[3:4] = jnp.concatenate([cg[...], cg[...]], axis=1)
 
-    pl.semaphore_wait(barrier, 8)
+    pl.semaphore_wait(barrier, 10)
 
     bufs = {"M": M, "G": G1, "H": G2, "D": D1, "E": D2}
     out_total = {"X1": X1.at[:7], "X2": X2.at[:7], "Q": preo, "R": rxo, "S": qo, "U": ro}
@@ -385,16 +401,15 @@
         nt = (((1,), (1,)), ((), ()))
         stat = (lax.dot_general(ones, high, nt, preferred_element_type=F32)
                 + lax.dot_general(ones, low, nt, preferred_element_type=F32))[:8]
-        scaled = (mixed * small[3:4]).astype(BF)
+        scaled = (mixed * small[3:4]).T.astype(BF)
         mixed_to[...] = scaled
         keep[0:8] = stat
 
     def mix_for(j):
-        nt = (((1,), (1,)), ((), ()))
         for mine in (False, True):
             core = c if mine else 1 - c
             w = M[lax.rem(x + j, 4), pl.ds(4 * core, 4), :, 128:].reshape(256, 128)
-            part = lax.dot_general(w, mixed_to[...], nt, preferred_element_type=F32)
+            part = jnp.dot(w, mixed_to[...], preferred_element_type=F32)
             if mine:
                 own32[j] = part
             else:
@@ -440,7 +455,8 @@
                 usc = jnp.concatenate([us[640:704].reshape(1, 64)] * 2, axis=1)
             gate = jnp.where(lane < 64, even, odd) * gsc
             up = pltpu.roll(jnp.where(lane < 64, odd, even), 64, axis=1) * usc
-            hid[:, 128 * n:128 * n + 128] = (gate / (1.0 + jnp.exp(-gate)) * up).astype(BF)
+            value = gate / (1.0 + jnp.exp(-gate)) * up
+            hid[128 * n:128 * n + 128] = value.T.astype(BF)
 
     def hidden_one():
         for n in range(4):
@@ -452,10 +468,15 @@
 
     def down(g, core):
         at = lax.rem(y + g, 4) + 4 * core
-        nt = (((1,), (1,)), ((), ()))
-        p = lax.dot_general(D1[:, at].reshape(256, D1L), hid[:, :D1L], nt, preferred_element_type=F32)
-        q = lax.dot_general(D2[:, at].reshape(256, D2L), hid[:, D1L:], nt, preferred_element_type=F32)
-        return (p + q).reshape(4, 64, T)
+        p = jnp.dot(D1[:, at, :64].reshape(256, D1L), hid[:D1L], preferred_element_type=F32)
+        q = jnp.dot(D2[:, at].reshape(256, D2L), hid[D1L:D1L + D2L], preferred_element_type=F32)
+        fold = [D1[:, at, 64:, 128 * k:128 * k + 128].astype(F32) for k in range(2)]
+        flat = []
+        for f in fold:
+            flat += [f, pltpu.roll(f.reshape(64, 128), 64, axis=1).reshape(4, 16, 128)]
+        tail = jnp.concatenate(flat, axis=1).reshape(256, 128).astype(BF)
+        r = jnp.dot(tail, hid[D1L + D2L:], preferred_element_type=F32)
+        return (p + q + r).reshape(4, 64, T)
 
     def down_partner(g):
         qo[g] = down(g, 1 - c).astype(BF)
@@ -509,8 +530,8 @@
     left()
 
 
-N_EVENTS = 12 + 40 + 12 + 12 + 40 + 7 + 4 + 3 + 7 + 4 + 12
-N_OUT, N_IN = 16, 107
+N_EVENTS = 18 + 40 + 18 + 18 + 40 + 7 + 4 + 3 + 7 + 4 + 12
+N_OUT, N_IN = 16, 125
 
 
 def local(residual, mixer_gain, value_weight, value_scale, input_gate_weight, input_gate_scale,
@@ -529,9 +550,9 @@
         out_specs=vmem,
         scratch_shapes=[
             V((4, 8, 64, NM), BF), V((4, 8, 64, G1L), BF), V((4, 8, 64, G2L), BF),
-            V((4, 8, 64, D1L), BF), V((4, 8, 64, D2L), BF),
-            V((8, T, 256), BF), V((8, T, 256), BF), V((T, 2048), BF), V((T, D1L + D2L), BF),
-            V((8, T), F32), V((T, 128), BF), V((4, 256, T), F32),
+            V((4, 8, DROWS, D1L), BF), V((4, 8, 64, D2L), BF),
+            V((8, T, 256), BF), V((8, T, 256), BF), V((T, 2048), BF), V((D1L + D2L + 128, T), BF),
+            V((8, T), F32), V((128, T), BF), V((4, 256, T), F32),
             V((4, ST, T), BF), V((4, ST, T), BF), V((3, ST, T), BF), V((3, ST, T), BF),
             V((4, 4, 64, T), BF), V((4, 4, 64, T), BF), V((4, 3, 64, T), BF), V((4, 3, 64, T), BF),
             V((256, T), BF), V((1, 2048), F32), V((1, 2048), F32), V((64, 64), F32), V((64, 64), F32),

time: 79.9 us -> 78.2 us (0.979)
  Pallas kernels: 79.1 us -> 77.3 us
    pallas_call x1, Pallas kernels: 79.1 us -> 77.3 us  [local(): pl.pallas_call(functools.partial(kernel, n_events=N_EVENTS), out_shape=V(...]
where the time goes in v5:
time: 78.2 us; the launch traced here: 78 us
  Pallas kernels  77.3 us (99%)
    pallas_call x1, Pallas kernels, local(): pl.pallas_call(functools.partial(kernel, n_events=N_EVENTS), out_shape=V(...  77.3 us

profile of v5, /device:TPU:1, one launch (start us, length us, event | category | flops | bytes accessed | tf_op | source)
XLA Modules:
  0.0 78.0 jit_solution(9743541129439746823)
XLA Ops:
  0.0 77.3 %layer.1 = f32[256,256]{1,0:T(8,128)S(1)} custom-call(bf16[256,256]{1,0:T(8,128)(2,1)} %res_in.1, f32[1,2048]{1,0:T(1,128)} %bitcast.10, f32[1,2048]{1,0:T(1,128)} %bitcast.11, f32[64,64]{1,0:T(8,128)} %v_in.1, f32[64,64]{1,0:T(8,128)} %i_in.1, f32[64,64]{1,0:T(8,128)} %o_in.1, f32[64,64]{1,0:T(8,128)} %w_in.1, f32[64,704]{1,0:T(8,128)} %g_in.1, ...), custom_call_target="tpu_custom_call" | custom-call | tf_op jit(solution)/shard_map/layer/pallas_call | solution.py:546
  77.3 0.7 convert_element_type.3
